TPU v7x, 256 devices: a 8x8x2 block of a 8x8x16 slice. The times are simulated.
256 devices in a mesh: grp: 2 (over z), sp: 16 (over y, core), tp: 8 (over x).
Axes of the slice: x: 8, y: 8, z: 2, core: 2. Of those that a mesh axis runs over, the one named last changes fastest.
The devices are a block of a 8x8x16 slice.
Arguments:
- residual: bfloat16 [32768, 2048], P(('grp', 'sp', 'tp')), parts along dimension 0, may hold values from -6 to 6
- grouped_value_heads: bfloat16 [32768, 2, 1024], P(('grp', 'sp'), None, 'tp'), parts along dimension 0, may hold values from -6 to 6
- output_gate_heads: bfloat16 [32768, 2, 1024], P(('grp', 'sp'), None, 'tp'), parts along dimension 0, may hold values from -6 to 6
- projected_key_query: bfloat16 [32768, 384], P(('grp', 'sp')), parts along dimension 0, may hold values from -6 to 6
- raw_step_size: bfloat16 [32768, 2, 16], P(('grp', 'sp'), None, 'tp'), parts along dimension 0, may hold values from -3 to 3
- step_size_bias: float32 [2, 16], P(None, 'tp'), may hold values from -1 to 0.5
- head_decay_logarithm: float32 [2, 16], P(None, 'tp'), may hold values from -16 to -2
- position_extra_decay: float32 [32768], P(('grp', 'sp')), parts along dimension 0, may hold values from -0.7 to 0
- head_skip_weight: float32 [2, 16], P(None, 'tp'), may hold values from 0.5 to 2
- value_kernel_taps: bfloat16 [4, 2, 1024], P(None, None, 'tp'), may hold values from -3 to 3
- key_query_kernel: bfloat16 [4, 384], replicated, may hold values from -3 to 3
- head_norm_gain: float32 [2, 1024], P(None, 'tp'), may hold values from 0.1 to 1.9
- output_matrix: bfloat16 [2, 1024, 2048], P(None, 'tp'), may hold values from -0.125 to 0.125
- expert_norm_gain: float32 [2048], replicated, may hold values from 0.1 to 1.9
- expert_gate_weight: bfloat16 [16, 2048, 4096], P('sp', None, 'tp'), may hold values from -0.125 to 0.125
- expert_up_weight: bfloat16 [16, 2048, 4096], P('sp', None, 'tp'), may hold values from -0.125 to 0.125
- expert_down_weight: bfloat16 [16, 4096, 2048], P('sp', 'tp'), may hold values from -0.09375 to 0.09375
- token_expert_choice: int32 [32768, 2], P(('grp', 'sp', 'tp')), parts along dimension 0, may hold values from 0 to 15, all different within a row; in each aligned block of 128 rows (0 to 127, 128 to 255, ...) at most 17 rows name the same one
- expert_output_weight: float32 [32768, 2], P(('grp', 'sp', 'tp')), parts along dimension 0, may hold values from 0.2 to 1
Outputs:
- layer_out: bfloat16 [32768, 2048], P(('grp', 'sp', 'tp')), parts along dimension 0
There are 2 independent parts, one for each index of `grp`. A program takes and returns all parts, laid end to end along the dimension named above; an argument that names none is the same for every part. Nothing has to cross between parts.
Inputs may be any that keep to these rules, and one draw needn't show every extreme that they name: `token_expert_choice`: each row names two different experts. The token rows of one device name one expert at most 17 times.
All inputs are finite; a program needn't handle non-finite values.
Results may differ from a plain program's by a relative error of at most 0.015.
Values may be sent and summed in bfloat16 or wider, within the bound.
A program may use at most 128 MiB of HBM per device.

v0:
```python
import functools
import types

import jax
import jax.numpy as jnp
from jax import lax
from jax.experimental import pallas as pl
from jax.experimental.pallas import tpu as pltpu
from jax.sharding import PartitionSpec as P

HEAD_DIM = 64
STATE_ONE = 64
STATE_TWO = 128
BLOCK = 128
EPSILON = 1e-06

MESH = pl.DeviceIdType.MESH
PIECE = 256
HEADS = 4
VMEM_LIMIT = 67043328


def remote(src, dst, send, recv, device):
    return pltpu.make_async_remote_copy(
        src_ref=src, dst_ref=dst, send_sem=send, recv_sem=recv, device_id=device, device_id_type=MESH
    )


def silu(a):
    return a * (1.0 / (1.0 + jnp.exp(-a)))


def layer_kernel(dims, names, *refs):
    r = types.SimpleNamespace(**dict(zip(names, refs, strict=True)))
    f32, bf16 = jnp.float32, jnp.bfloat16
    places, columns, width, rows = dims.places, dims.columns, dims.width, BLOCK
    half, chips, blocks = columns // 2, places // 2, columns
    me_x, me_s = lax.axis_index("tp"), lax.axis_index("sp")
    core, me_y = lax.rem(me_s, 2), lax.div(me_s, 2)
    right = {"tp": lax.rem(me_x + 1, columns)}
    left = {"tp": lax.rem(me_x + columns - 1, columns)}
    mate = {"sp": me_s + 1 - 2 * core}
    following = {"sp": lax.rem(me_s + 1, places)}

    def column(offset):
        return lax.rem(me_x + offset + columns, columns)

    def place(offset):
        return lax.rem(me_s + offset, places)

    def peer(offset):
        return {"sp": lax.rem(me_s + 2 * offset, places)}

    def toward(way):
        return right if way == 0 else left

    loads = [
        (r.matrix_hbm.at[0], r.matrix.at[me_x, pl.ds(0, rows), :]),
        (r.matrix_hbm.at[1], r.matrix.at[me_x, pl.ds(rows, rows), :]),
        (r.value_hbm, r.value_in),
        (r.keys_hbm, r.keys_in),
        (r.gate_hbm, r.gate_in),
    ]
    early = len(loads)
    for t in range(dims.tiles):
        span = pl.ds(t * 128, 128)
        loads.append((r.expert_gate_hbm.at[0, :, span], r.gate_up.at[t, :, pl.ds(0, 128)]))
        loads.append((r.expert_up_hbm.at[0, :, span], r.gate_up.at[t, :, pl.ds(128, 128)]))
    for p in range(dims.pieces):
        loads.append((r.expert_down_hbm.at[0, :, pl.ds(p * PIECE, PIECE)], r.down.at[p]))
    loads = [pltpu.make_async_copy(a, b, r.load_sem.at[n]) for n, (a, b) in enumerate(loads)]
    for load in loads:
        load.start()

    barrier = pltpu.get_barrier_semaphore()
    peers = [{"tp": column(i)} for i in range(1, columns)] + [{"sp": place(i)} for i in range(1, places)]
    for device in peers:
        pl.semaphore_signal(barrier, inc=1, device_id=device, device_id_type=MESH)

    for g in range(2):
        raw = r.raw_ref[g].astype(f32)
        for k in range(blocks):
            r.stride_s[HEADS * k + 2 * g : HEADS * k + 2 * g + 2, :] = raw[:, k * rows : (k + 1) * rows]
    for k in range(blocks):
        r.run_s[HEADS * k : HEADS * k + HEADS, :] = jnp.broadcast_to(r.extra_ref[k : k + 1, :], (HEADS, rows))
    head_of = jnp.bitwise_and(lax.broadcasted_iota(jnp.int32, (HEADS * blocks, rows), 0), HEADS - 1)

    def by_head(table):
        picked = jnp.full((HEADS * blocks, rows), table[1, 1], f32)
        for n in range(3):
            picked = jnp.where(head_of == n, table[n // 2, n % 2], picked)
        return picked

    shifted = r.stride_s[...] + by_head(r.bias_ref)
    stride = jnp.maximum(shifted, 0.0) + jnp.log1p(jnp.exp(-jnp.abs(shifted)))
    log_decay = r.run_s[...] - jnp.exp(by_head(r.log_ref)) * stride
    at_row = lax.broadcasted_iota(jnp.int32, (rows, rows), 0)
    at_lane = lax.broadcasted_iota(jnp.int32, (rows, rows), 1)
    running = jnp.dot(
        log_decay,
        jnp.where(at_row <= at_lane, 1.0, 0.0),
        preferred_element_type=f32,
        precision=lax.Precision.HIGHEST,
    )
    ends = jnp.broadcast_to(running[:, rows - 1 : rows], running.shape)
    r.stride_s[...] = stride
    r.run_s[...] = running
    r.fade_s[...] = jnp.exp(ends - running) * stride
    r.end_s[...] = jnp.exp(ends)
    turned = jnp.transpose(running)
    for k in range(blocks):
        r.cols_s[k, :, 0:HEADS] = turned[:, HEADS * k : HEADS * k + HEADS]

    first_head = at_lane < HEAD_DIM

    def row_pair(table, k, g):
        low = table[pl.ds(HEADS * k + 2 * g, 1), :]
        high = table[pl.ds(HEADS * k + 2 * g + 1, 1), :]
        return jnp.where(first_head[0:1], low, high)

    r.tables[me_x] = jnp.zeros((8, rows), f32)
    r.tables[me_x, 0:2, :] = r.choice_ref[...].astype(f32)
    r.tables[me_x, 2:4, :] = r.share_ref[...]

    for load in loads[: early - 1]:
        load.wait()
    pl.semaphore_wait(barrier, len(peers))

    cut = width // 2
    mine = pl.ds(pl.multiple_of(core * rows, rows), rows)

    def matrix_ring(way, event, col):
        here = r.matrix.at[col, mine, pl.ds(((event % 2) ^ way) * cut, cut)]
        return remote(here, here, r.ring_send.at[way, event], r.ring_recv.at[way, event], toward(way))

    def matrix_pass(way, event, col):
        here = r.matrix.at[col, mine, pl.ds(((event % 2) ^ way) * cut, cut)]
        return remote(here, here, r.pass_send.at[way, event], r.pass_recv.at[way, event], mate)

    rim_rows = 16
    positions = blocks * rows
    rims = [
        remote(
            r.value_in.at[pl.ds(2 * positions - rim_rows, rim_rows), :],
            r.value_rim,
            r.rim_send.at[0],
            r.rim_recv.at[0],
            following,
        ),
        remote(
            r.keys_in.at[pl.ds(positions - rim_rows, rim_rows), :], r.keys_rim, r.rim_send.at[1], r.rim_recv.at[1], following
        ),
    ]
    for rim in rims:
        rim.start()

    def table_copy(offset):
        return remote(
            r.tables.at[me_x],
            r.tables.at[me_x],
            r.table_send.at[offset],
            r.table_recv.at[columns - offset],
            {"tp": column(offset)},
        )

    for i in range(1, columns):
        table_copy(i).start()
    for event in range(2):
        for way in range(2):
            if event < columns - 1:
                matrix_ring(way, event, me_x).start()

    def service(event):
        k = event // 2 + 1
        for way in range(2):
            col = column(-k if way == 0 else k)
            matrix_ring(way, event, col).wait_recv()
            if event + 2 < columns - 1:
                matrix_ring(way, event + 2, col).start()
            matrix_pass(way, event, col).start()

    r.value_wide[rim_rows:, :] = r.value_in[...].astype(f32)
    r.keys_wide[rim_rows:, :] = r.keys_in[...].astype(f32)
    taps = r.value_tap_ref.shape[0] // 2
    value_tap = r.value_tap_ref[...].astype(f32)
    key_tap = r.key_tap_ref[...].astype(f32)
    even = jnp.bitwise_and(lax.broadcasted_iota(jnp.int32, (2 * rows, rows), 0), 1) == 0
    tap_rows = [jnp.where(even, value_tap[2 * j : 2 * j + 1], value_tap[2 * j + 1 : 2 * j + 2]) for j in range(taps)]

    def states_of(k):
        window = r.value_wide[pl.ds(pl.multiple_of(k * 2 * rows, 2 * rows), 2 * rows + rim_rows), :]
        total = jnp.zeros((2 * rows, rows), f32)
        for j in range(taps):
            start = rim_rows - 2 * (taps - 1 - j)
            total = total + window[start : start + 2 * rows] * tap_rows[j]
        r.conv_wide[...] = silu(total).astype(bf16).astype(f32)
        window = r.keys_wide[pl.ds(pl.multiple_of(k * rows, rows), rows + rim_rows), :]
        total = jnp.zeros((rows, r.keys_wide.shape[1]), f32)
        for j in range(taps):
            start = rim_rows - (taps - 1 - j)
            total = total + window[start : start + rows] * key_tap[j : j + 1]
        conv = silu(total).astype(bf16).astype(f32)
        both = conv[:, 0 : 2 * STATE_ONE]
        keys = [jnp.where(first_head, both, 0.0), conv[:, 2 * STATE_ONE : 2 * STATE_ONE + STATE_TWO]]
        asks = [pltpu.roll(both, STATE_ONE, 1), conv[:, 2 * STATE_ONE + STATE_TWO :]]
        for g in range(2):
            x = r.conv_wide[pl.ds(g, rows, stride=2), :].astype(bf16)
            key_t = jnp.transpose(keys[g])
            r.x_s[k, g] = x
            r.kt_s[k, g] = key_t.astype(bf16)
            r.q_s[k, g] = asks[g].astype(bf16)
            faded = jnp.concatenate(
                [key_t * r.fade_s[pl.ds(HEADS * k + 2 * g + h, 1), :] for h in range(2)], axis=0
            ).astype(bf16)
            state = jnp.dot(faded, x, preferred_element_type=f32)
            r.state_s[k, g] = jnp.where(first_head, state[:rows], state[rows:])

    def state_step(i, carry):
        states_of(i)
        return carry

    lax.fori_loop(1, blocks, state_step, 0)
    for rim in rims:
        rim.wait_recv()
    opening = me_s == 0
    r.value_wide[0:rim_rows, :] = jnp.where(opening, 0.0, r.value_rim[...].astype(f32))
    r.keys_wide[0:rim_rows, :] = jnp.where(opening, 0.0, r.keys_rim[...].astype(f32))
    states_of(0)

    packed = STATE_TWO + STATE_ONE
    piece = packed // 2

    def local_end(g):
        total = jnp.zeros((rows, rows), f32)
        faded = jnp.ones((1, rows), f32)
        for k in range(blocks):
            decay = row_pair(r.end_s, k, g)
            total = total * decay + r.state_s[k, g]
            faded = faded * decay
        return total, faded

    end_one, fade_one = local_end(0)
    end_two, fade_two = local_end(1)
    own = jnp.concatenate([end_two, end_one[:STATE_ONE]], axis=0)
    r.own_pack[...] = own.astype(bf16)
    r.own_fade[0:1, :] = fade_one
    r.own_fade[1:2, :] = fade_two
    r.own_fade[2:8, :] = jnp.zeros((6, rows), f32)
    mates = [
        remote(r.own_pack, r.mate_pack, r.mate_send.at[0], r.mate_recv.at[0], mate),
        remote(r.own_fade, r.mate_fade, r.mate_send.at[1], r.mate_recv.at[1], mate),
    ]
    for copy in mates:
        copy.start()
    service(0)
    for copy in mates:
        copy.wait_recv()
    is_low = core == 0
    low = jnp.where(is_low, own, r.mate_pack[...].astype(f32))
    high = jnp.where(is_low, r.mate_pack[...].astype(f32), own)
    mate_rows = r.mate_fade[...]
    own_rows = r.own_fade[...]
    high_rows = jnp.where(is_low, mate_rows, own_rows)
    in_two = lax.broadcasted_iota(jnp.int32, (packed, rows), 0) < STATE_TWO
    r.chip_pack[...] = (low * jnp.where(in_two, high_rows[1:2], high_rows[0:1]) + high).astype(bf16)
    r.chip_fade[...] = own_rows * mate_rows
    my_half = pl.ds(pl.multiple_of(core * piece, 16), piece)

    def to_chip(n, which):
        src = r.chip_pack.at[my_half, :] if which == 0 else r.chip_fade
        dst = r.all_pack.at[me_y] if which == 0 else r.all_fade.at[me_y]
        return remote(src, dst, r.chip_send.at[which, n], r.chip_recv.at[which, n], peer(n))

    for n in range(1, chips):
        for which in range(2):
            to_chip(n, which).start()

    below = at_row >= at_lane

    def near_step(k, carry):
        cols = r.cols_s[k]
        for g in range(2):
            scores = jnp.dot(r.q_s[k, g], r.kt_s[k, g], preferred_element_type=f32)
            parts = []
            for h in range(2):
                n = 2 * g + h
                gap = cols[:, n : n + 1] - r.run_s[pl.ds(HEADS * k + n, 1), :]
                damping = jnp.exp(jnp.where(below, gap, -1e30))
                parts.append((scores * damping * r.stride_s[pl.ds(HEADS * k + n, 1), :]).astype(bf16))
            near = jnp.dot(jnp.concatenate(parts, axis=0), r.x_s[k, g], preferred_element_type=f32)
            r.near_s[k, g] = jnp.where(first_head, near[:rows], near[rows:])
        return carry

    lax.fori_loop(0, blocks, near_step, 0)
    if columns > 2:
        service(1)
    loads[early - 1].wait()

    for n in range(1, chips):
        for which in range(2):
            to_chip(n, which).wait_recv()
    row_at = lax.broadcasted_iota(jnp.int32, (piece, rows), 0) + core * piece
    half_two = row_at < STATE_TWO
    entering = jnp.zeros((piece, rows), f32)
    for y in range(chips):
        fades = r.all_fade[y]
        later = entering * jnp.where(half_two, fades[1:2], fades[0:1]) + r.all_pack[y].astype(f32)
        entering = jnp.where(y < me_y, later, entering)
    r.enter_pack[my_half, :] = entering.astype(bf16)
    here = r.enter_pack.at[my_half, :]
    enter_copy = remote(here, here, r.enter_send.at[0], r.enter_recv.at[0], mate)
    enter_copy.start()
    enter_copy.wait_recv()
    chip_state = r.enter_pack[...].astype(f32)
    after_low = chip_state * jnp.where(in_two, mate_rows[1:2], mate_rows[0:1]) + r.mate_pack[...].astype(f32)
    entered = jnp.where(is_low, chip_state, after_low)
    r.carry_s[1] = entered[:STATE_TWO]
    r.carry_s[0] = jnp.zeros((rows, rows), f32)
    r.carry_s[0, 0:STATE_ONE, :] = entered[STATE_TWO:]

    def head_copy(col):
        return remote(r.mixed_s.at[col], r.heads_in.at[me_x], r.head_send.at[col], r.head_recv.at[me_x], {"tp": col})

    def mix_step(k, carry):
        cols = jnp.exp(r.cols_s[k])
        r.gate_wide[...] = r.gate_in[pl.ds(pl.multiple_of(k * 2 * rows, 2 * rows), 2 * rows), :].astype(f32)
        for g in range(2):
            state = r.carry_s[g]
            coarse = state.astype(bf16)
            fine = (state - coarse.astype(f32)).astype(bf16)
            ask = r.q_s[k, g]
            far = jnp.dot(
                jnp.concatenate([ask, ask], axis=1),
                jnp.concatenate([coarse, fine], axis=0),
                preferred_element_type=f32,
            )
            reach = jnp.where(first_head, cols[:, 2 * g : 2 * g + 1], cols[:, 2 * g + 1 : 2 * g + 2])
            skip = jnp.where(first_head[0:1], r.skip_ref[g, 0], r.skip_ref[g, 1])
            mixed = r.near_s[k, g] + far * reach + skip * r.x_s[k, g].astype(f32)
            gated = mixed * silu(r.gate_wide[pl.ds(g, rows, stride=2), :])
            square = gated * gated
            one = jnp.sum(jnp.where(first_head, square, 0.0), axis=1, keepdims=True)
            two = jnp.sum(jnp.where(first_head, 0.0, square), axis=1, keepdims=True)
            scale = lax.rsqrt(jnp.where(first_head, one, two) * (1.0 / HEAD_DIM) + EPSILON)
            r.mixed_s[k, :, g * rows : (g + 1) * rows] = (gated * scale * r.head_gain_ref[g : g + 1, :]).astype(bf16)
            r.carry_s[g] = state * row_pair(r.end_s, k, g) + r.state_s[k, g]

        @pl.when(k != me_x)
        def _():
            head_copy(k).start()

        return carry

    lax.fori_loop(0, blocks, mix_step, 0)
    r.heads_in[me_x] = r.mixed_s[me_x]

    main, over, slots = dims.main, dims.over, places * dims.main
    total_slots = slots + over
    slot_row = lax.broadcasted_iota(jnp.int32, (total_slots, over), 0)
    slot_expert = lax.broadcasted_iota(jnp.int32, (total_slots, over), 1)
    spread = jnp.where(
        ((slot_row < slots) & (slot_row >= slot_expert * main) & (slot_row < slot_expert * main + main))
        | (slot_row == slots + slot_expert),
        1.0,
        0.0,
    ).astype(bf16)
    at = lax.broadcasted_iota(jnp.int32, (total_slots, rows), 0)
    turn = jnp.where(at < slots, jnp.bitwise_and(at, main - 1), main).astype(f32)
    expert_at = lax.broadcasted_iota(jnp.int32, (over, rows), 0).astype(f32)
    earlier = jnp.where(at_row < at_lane, 1.0, 0.0).astype(bf16)

    def make_put(col):
        table = r.tables[col]
        named = jnp.where((expert_at == table[0:1]) | (expert_at == table[1:2]), 1.0, 0.0)
        rank = jnp.dot(named.astype(bf16), earlier, preferred_element_type=f32)
        named_x = jnp.dot(spread, named.astype(bf16), preferred_element_type=f32)
        rank_x = jnp.dot(spread, rank.astype(bf16), preferred_element_type=f32)
        r.put[col] = jnp.where(rank_x == turn, named_x, 0.0).astype(bf16)

    for i in range(1, columns):
        table_copy(i).wait_recv()

    def put_step(col, carry):
        make_put(col)
        return carry

    lax.fori_loop(0, columns, put_step, 0)

    slot_col = lax.broadcasted_iota(jnp.int32, (over, total_slots), 1)
    slot_exp = lax.broadcasted_iota(jnp.int32, (over, total_slots), 0)
    spread_t = jnp.where(
        ((slot_col < slots) & (slot_col >= slot_exp * main) & (slot_col < slot_exp * main + main))
        | (slot_col == slots + slot_exp),
        1.0,
        0.0,
    ).astype(bf16)
    at_t = lax.broadcasted_iota(jnp.int32, (rows, total_slots), 1)
    turn_t = jnp.where(at_t < slots, jnp.bitwise_and(at_t, main - 1), main).astype(f32)
    expert_to = lax.broadcasted_iota(jnp.int32, (rows, over), 1).astype(f32)
    later_t = jnp.where(at_lane < at_row, 1.0, 0.0).astype(bf16)

    def make_pick(col):
        table = jnp.transpose(r.tables[col])
        named = [jnp.where(expert_to == table[:, k : k + 1], 1.0, 0.0) for k in range(2)]
        rank = jnp.dot(later_t, (named[0] + named[1]).astype(bf16), preferred_element_type=f32)
        rank_x = jnp.dot(rank.astype(bf16), spread_t, preferred_element_type=f32)
        for k in range(2):
            named_x = jnp.dot(named[k].astype(bf16), spread_t, preferred_element_type=f32)
            r.pick[col, k] = jnp.where(rank_x == turn_t, named_x, 0.0).astype(bf16)
            r.share_s[col, k] = jnp.broadcast_to(table[:, 2 + k : 3 + k], (rows, rows))

    def arrived(col):
        return remote(r.mixed_s.at[col], r.heads_in.at[col], r.head_send.at[col], r.head_recv.at[col], {"tp": col})

    def product(col, first=False):
        for n in range(0, width, 512):
            part = jnp.dot(r.heads_in[col], r.matrix[col, :, n : n + 512], preferred_element_type=f32)
            r.acc_s[:, n : n + 512] = part if first else r.acc_s[:, n : n + 512] + part

    product(me_x, True)
    for event in range(2, columns - 1):
        service(event)
    for k in range(1, half + 1):
        for way in range(2):
            if way == 1 and k == half:
                continue
            for event in (2 * k - 2, 2 * k - 1):
                if event < columns - 1:
                    for side in range(2) if k == half else (way,):
                        matrix_pass(side, event, column(k if side else -k)).wait_recv()
            col = column(-k if way == 0 else k)
            arrived(col).wait_recv()
            product(col)

    stream = (r.residual_ref[...].astype(f32) + r.acc_s[...]).astype(bf16)
    r.stream_s[...] = stream
    wide = stream.astype(f32)
    scale = lax.rsqrt(jnp.mean(wide * wide, axis=1, keepdims=True) + EPSILON)
    normed = (wide * scale * r.expert_gain_ref[...]).astype(bf16)

    direct, extra = dims.direct, dims.pieces - dims.direct
    pieces = dims.pieces
    lanes_of = PIECE // 128

    def lines(index):
        return pl.ds(pl.multiple_of(index * main, main), main)

    def far(way, p):
        odd = lax.rem(p, 2) if not isinstance(p, int) else p % 2
        return half - odd if way == 0 else half - 1 + odd

    for q in range(extra):
        r.tokens[me_x, q] = normed[:, (direct + q) * PIECE : (direct + q + 1) * PIECE]

    def token_ring(way, step, q, col):
        here = r.tokens.at[col, q]
        return remote(here, here, r.token_send.at[way, step, q], r.token_recv.at[way, step, q], toward(way))

    put_own = r.put[me_x]
    for p in range(direct):
        part = jnp.dot(put_own, normed[:, p * PIECE : (p + 1) * PIECE], preferred_element_type=f32)
        r.outbound[p] = part[:slots].astype(bf16)
        for c in range(lanes_of):
            r.over_out[:, p * lanes_of + c, :] = part[slots:, c * 128 : (c + 1) * 128]
    for q in range(extra):
        for way in range(2):
            token_ring(way, 0, q, me_x).start()

    for i in range(1, places):
        remote(
            r.over_out.at[place(i)], r.over_in.at[me_s], r.over_send.at[0], r.over_recv.at[0], {"sp": place(i)}
        ).start()

    def send_out(p, carry):
        for i in range(1, places):
            remote(
                r.outbound.at[p, lines(place(i)), :],
                r.chunks.at[me_x, p, lines(me_s), :],
                r.out_send.at[p],
                r.out_recv.at[p],
                {"sp": place(i)},
            ).start()
        r.chunks[me_x, p, lines(me_s), :] = r.outbound[p, lines(me_s), :]
        return carry

    lax.fori_loop(0, direct, send_out, 0)
    r.over_in[me_s] = r.over_out[me_s]
    if places < over:
        r.over_in[places:over] = jnp.zeros((over - places, *r.over_in.shape[1:]), f32)
        r.over_ret[places:over] = jnp.zeros((over - places, *r.over_ret.shape[1:]), f32)
        r.xover_in[:, places:over] = jnp.zeros((columns, over - places, *r.xover_in.shape[2:]), f32)
        r.xover_ret[:, places:over] = jnp.zeros((columns, over - places, *r.xover_ret.shape[2:]), f32)

    def route(offset):
        col = column(offset)
        for q in range(extra):
            part = jnp.dot(r.put[col], r.tokens[col, q], preferred_element_type=f32)
            r.xout[col, q] = part[:slots].astype(bf16)
            r.chunks[col, direct + q, lines(me_s), :] = r.xout[col, q, lines(me_s), :]
            for c in range(lanes_of):
                r.xover_out[offset, :, q * lanes_of + c, :] = part[slots:, c * 128 : (c + 1) * 128]
        r.xover_in[offset, me_s] = r.xover_out[offset, me_s]
        for i in range(1, places):
            remote(
                r.xout.at[col, :, lines(place(i)), :],
                r.chunks.at[col, pl.ds(direct, extra), lines(me_s), :],
                r.xout_send.at[offset],
                r.xout_recv.at[offset],
                {"sp": place(i)},
            ).start()
            remote(
                r.xover_out.at[offset, place(i)],
                r.xover_in.at[offset, me_s],
                r.xover_send.at[0, offset],
                r.xover_recv.at[0, offset],
                {"sp": place(i)},
            ).start()

    def routed(offset):
        col = column(offset)
        most = pl.ds(0, (places - 1) * main)
        return (
            remote(
                r.xout.at[col, :, most, :],
                r.chunks.at[col, pl.ds(direct, extra), most, :],
                r.xout_send.at[offset],
                r.xout_recv.at[offset],
                right,
            ),
            remote(
                r.xover_out.at[offset, 0 : places - 1],
                r.xover_in.at[offset, 0 : places - 1],
                r.xover_send.at[0, offset],
                r.xover_recv.at[0, offset],
                right,
            ),
        )

    def take_routed(offset):
        col = column(offset)
        for copy in routed(offset):
            copy.wait_recv()
        for q in range(extra):
            for c in range(lanes_of):
                r.chunks[col, direct + q, slots:, c * 128 : (c + 1) * 128] = r.xover_in[
                    offset, :, q * lanes_of + c, :
                ].astype(bf16)

    route(0)

    def token_event(k):
        for q in range(extra):
            for way in range(2):
                if k <= far(way, q):
                    col = column(-k if way == 0 else k)
                    token_ring(way, k - 1, q, col).wait_recv()
                    if k < far(way, q):
                        token_ring(way, k, q, col).start()
        if k < half:
            route(columns - k)
        route(k)

    def chunk_ring(way, step, p, col):
        here = r.chunks.at[col, p]
        return remote(here, here, r.chunk_send.at[way, step, p], r.chunk_recv.at[way, step, p], toward(way))

    def out_arrived(p):
        most = pl.ds(0, (places - 1) * main)
        return remote(
            r.outbound.at[p, most, :], r.chunks.at[me_x, p, most, :], r.out_send.at[p], r.out_recv.at[p], right
        )

    def start_piece(p):
        out_arrived(p).wait_recv()
        chunk_ring(0, 0, p, me_x).start()
        chunk_ring(1, 0, p, me_x).start()

    remote(
        r.over_out.at[0 : places - 1], r.over_in.at[0 : places - 1], r.over_send.at[0], r.over_recv.at[0], right
    ).wait_recv()
    for c in range(direct * lanes_of):
        at_lanes = (c % lanes_of) * 128
        r.chunks[me_x, c // lanes_of, slots:, at_lanes : at_lanes + 128] = r.over_in[:, c, :].astype(bf16)
    for n in range(max(direct, half)):
        if n < direct:
            start_piece(n)
        if n < half:
            token_event(n + 1)

    def offset_of(n):
        k = lax.div(n + 1, 2)
        return jnp.where(lax.rem(n, 2) == 1, lax.rem(columns - k, columns), k)

    def unit(n, t):
        offset = offset_of(n)
        col = column(offset)
        pl.when(t == 0)(lambda: take_routed(offset))
        acc = jnp.dot(r.chunks[col, 0], r.gate_up[t, 0:PIECE, :], preferred_element_type=f32)
        for q in range(1, pieces):
            acc = acc + jnp.dot(
                r.chunks[col, q], r.gate_up[t, q * PIECE : (q + 1) * PIECE, :], preferred_element_type=f32
            )
        value = silu(acc[:, 0:128]) * acc[:, 128:256]
        r.hidden[col, :, pl.ds(pl.multiple_of(t * 128, 128), 128)] = value.astype(bf16)
        pl.when(t == dims.tiles - 1)(lambda: give_back(offset))

    def own(col, p):
        return jnp.dot(r.hidden[col], r.down[p], preferred_element_type=f32)

    def give_back(offset):
        col = column(offset)
        for q in range(extra):
            part = own(col, direct + q)
            r.xback[col, q] = part[:slots].astype(bf16)
            r.xret[col, q, lines(me_s), :] = r.xback[col, q, lines(me_s), :]
            for c in range(lanes_of):
                r.xover_back[offset, :, q * lanes_of + c, :] = part[slots:, c * 128 : (c + 1) * 128]
        r.xover_ret[offset, me_s] = r.xover_back[offset, me_s]
        for i in range(1, places):
            remote(
                r.xback.at[col, :, lines(place(i)), :],
                r.xret.at[col, :, lines(me_s), :],
                r.xback_send.at[offset],
                r.xback_recv.at[offset],
                {"sp": place(i)},
            ).start()
            remote(
                r.xover_back.at[offset, place(i)],
                r.xover_ret.at[offset, me_s],
                r.xover_send.at[1, offset],
                r.xover_recv.at[1, offset],
                {"sp": place(i)},
            ).start()

    def given_back(offset):
        col = column(offset)
        most = pl.ds(0, (places - 1) * main)
        return (
            remote(
                r.xback.at[col, :, most, :],
                r.xret.at[col, :, most, :],
                r.xback_send.at[offset],
                r.xback_recv.at[offset],
                right,
            ),
            remote(
                r.xover_back.at[offset, 0 : places - 1],
                r.xover_ret.at[offset, 0 : places - 1],
                r.xover_send.at[1, offset],
                r.xover_recv.at[1, offset],
                right,
            ),
        )

    for load in loads[early:]:
        load.wait()

    def units(low, high):
        def body(v, carry):
            unit(lax.div(v, dims.tiles), lax.rem(v, dims.tiles))
            return carry

        lax.fori_loop(low, high, body, 0)

    share_of = dims.schedule
    for k in range(1, half + 1):
        first, last = share_of[k - 1] * dims.tiles, share_of[k] * dims.tiles

        def pass_on(p, carry, k=k, first=first, last=last):
            for way in range(2):
                col = column(-k if way == 0 else k)

                @pl.when(k <= far(way, p))
                def _():
                    chunk_ring(way, k - 1, p, col).wait_recv()

                if k < half:

                    @pl.when(k < far(way, p))
                    def _():
                        chunk_ring(way, k, p, col).start()

            if last > first:
                units(
                    first + lax.div(p * (last - first), direct), first + lax.div((p + 1) * (last - first), direct)
                )
            return carry

        lax.fori_loop(0, direct, pass_on, 0)
        if k == 1:
            lax.fori_loop(0, columns, lambda col, carry: (make_pick(col), carry)[1], 0)
    units(share_of[half] * dims.tiles, columns * dims.tiles)

    def hop(way, j, p):
        buffer = r.sum_right if way == 0 else r.sum_left
        return remote(
            buffer.at[j, p],
            buffer.at[j - 1, p],
            r.sum_send.at[way, j - 1, p],
            r.sum_recv.at[way, j - 1, p],
            toward(way),
        )

    def round_of(t, low_piece, high_piece):
        def body(p, carry):
            for way in range(2):
                buffer = r.sum_right if way == 0 else r.sum_left
                j = far(1 - way, p) - t

                def work(way=way, buffer=buffer, j=j):
                    value = own(column(j if way == 0 else -j), p)
                    if t > 0:
                        hop(way, j + 1, p).wait_recv()
                        value = value + buffer[j, p].astype(f32)
                    buffer[j, p] = value.astype(bf16)
                    hop(way, j, p).start()

                if t < half - 1:
                    work()
                else:
                    pl.when(j >= 1)(work)
            return carry

        lax.fori_loop(low_piece, high_piece, body, 0)

    def finish(p, carry):
        value = own(me_x, p)
        hop(0, 1, p).wait_recv()
        hop(1, 1, p).wait_recv()
        value = value + r.sum_right[0, p].astype(f32) + r.sum_left[0, p].astype(f32)
        r.totals[p] = value[0:slots].astype(bf16)
        r.over_total[p] = value[slots:]
        r.returned[p, lines(me_s), :] = r.totals[p, lines(me_s), :]
        for i in range(1, places):
            remote(
                r.totals.at[p, lines(place(i)), :],
                r.returned.at[p, lines(me_s), :],
                r.back_send.at[p],
                r.back_recv.at[p],
                {"sp": place(i)},
            ).start()
        return carry

    def weighted(col, table, q):
        one = jnp.dot(r.pick[col, 0], table[q], preferred_element_type=f32)
        two = jnp.dot(r.pick[col, 1], table[q], preferred_element_type=f32)
        first, second = r.share_s[col, 0], r.share_s[col, 1]
        return jnp.concatenate([first] * lanes_of, axis=1) * one + jnp.concatenate([second] * lanes_of, axis=1) * two

    def take_back(offset):
        col = column(offset)
        for copy in given_back(offset):
            copy.wait_recv()
        for q in range(extra):
            for c in range(lanes_of):
                r.xret[col, q, slots:, c * 128 : (c + 1) * 128] = r.xover_ret[
                    offset, :, q * lanes_of + c, :
                ].astype(bf16)

    def token_hop(way, j, q):
        buffer = r.xsum_right if way == 0 else r.xsum_left
        return remote(
            buffer.at[j, q],
            buffer.at[j - 1, q],
            r.xsum_send.at[way, j - 1, q],
            r.xsum_recv.at[way, j - 1, q],
            toward(way),
        )

    taken = set()

    def token_round(t):
        for q in range(extra):
            for way in range(2):
                buffer = r.xsum_right if way == 0 else r.xsum_left
                j = far(1 - way, q) - t
                if j < 1:
                    continue
                offset = j if way == 0 else columns - j
                if offset not in taken:
                    taken.add(offset)
                    take_back(offset)
                col = column(offset)
                value = weighted(col, r.xret.at[col], q)
                if t > 0:
                    token_hop(way, j + 1, q).wait_recv()
                    value = value + buffer[j, q].astype(f32)
                buffer[j, q] = value.astype(bf16)
                token_hop(way, j, q).start()

    for t in range(half - 1):
        round_of(t, 0, direct)
    token_round(0)
    round_of(half - 1, 0, direct)
    if half > 1:
        token_round(1)
    lax.fori_loop(0, direct, finish, 0)
    for c in range(direct * lanes_of):
        at_lanes = (c % lanes_of) * 128
        r.over_back[:, c, :] = r.over_total[c // lanes_of, :, at_lanes : at_lanes + 128]
    r.over_ret[me_s] = r.over_back[me_s]
    for i in range(1, places):
        remote(
            r.over_back.at[place(i)], r.over_ret.at[me_s], r.over_send.at[1], r.over_recv.at[1], {"sp": place(i)}
        ).start()
    for t in range(2, half):
        token_round(t)
    take_back(0)
    for q in range(extra):
        value = weighted(me_x, r.xret.at[me_x], q)
        for way in range(2):
            token_hop(way, 1, q).wait_recv()
        value = value + r.xsum_right[0, q].astype(f32) + r.xsum_left[0, q].astype(f32)
        span = slice((direct + q) * PIECE, (direct + q + 1) * PIECE)
        r.out_ref[:, span] = (r.stream_s[:, span].astype(f32) + value).astype(bf16)

    remote(
        r.over_back.at[0 : places - 1], r.over_ret.at[0 : places - 1], r.over_send.at[1], r.over_recv.at[1], right
    ).wait_recv()
    for c in range(direct * lanes_of):
        at_lanes = (c % lanes_of) * 128
        r.returned[c // lanes_of, slots:, at_lanes : at_lanes + 128] = r.over_ret[:, c, :].astype(bf16)

    def back_arrived(p):
        most = pl.ds(0, (places - 1) * main)
        return remote(
            r.totals.at[p, most, :], r.returned.at[p, most, :], r.back_send.at[p], r.back_recv.at[p], right
        )

    def combine(p, carry):
        back_arrived(p).wait_recv()
        span = pl.ds(pl.multiple_of(p * PIECE, PIECE), PIECE)
        value = weighted(me_x, r.returned, p)
        r.out_ref[:, span] = (r.stream_s[:, span].astype(f32) + value).astype(bf16)
        return carry

    lax.fori_loop(0, direct, combine, 0)

    for copy in rims + mates + [enter_copy]:
        copy.wait_send()
    for n in range(1, chips):
        for which in range(2):
            to_chip(n, which).wait_send()
    for i in range(1, columns):
        head_copy(column(i)).wait_send()
        table_copy(i).wait_send()
    for event in range(columns - 1):
        for way in range(2):
            matrix_ring(way, event, me_x).wait_send()
            matrix_pass(way, event, me_x).wait_send()
    for n, (a, b) in enumerate(((r.over_out, r.over_in), (r.over_back, r.over_ret))):
        remote(a.at[0 : places - 1], b.at[0 : places - 1], r.over_send.at[n], r.over_recv.at[n], right).wait_send()
    for q in range(extra):
        for way in range(2):
            for k in range(far(way, q)):
                token_ring(way, k, q, me_x).wait_send()
            for k in range(far(1 - way, q)):
                token_hop(way, k + 1, q).wait_send()

    def drain_columns(offset, carry):
        for copy in routed(offset) + given_back(offset):
            copy.wait_send()
        return carry

    lax.fori_loop(0, columns, drain_columns, 0)

    def drain(p, carry):
        out_arrived(p).wait_send()
        back_arrived(p).wait_send()
        for way in range(2):
            for k in range(half):
                pl.when(k < far(way, p))(lambda way=way, k=k: chunk_ring(way, k, p, me_x).wait_send())
                pl.when(k < far(1 - way, p))(lambda way=way, k=k: hop(way, k + 1, p).wait_send())
        return carry

    lax.fori_loop(0, direct, drain, 0)


def layer(places, columns, **given):
    f32, bf16 = jnp.float32, jnp.bfloat16
    rows, width = given["residual_ref"].shape
    units = given["expert_gate_hbm"].shape[2]
    lanes = given["keys_hbm"].shape[1]
    positions = columns * BLOCK
    half, chips, blocks = columns // 2, places // 2, columns
    main = 2 * rows // places
    over = -(-places // 16) * 16
    pieces = width // PIECE
    extra = max(1, pieces // 4)
    direct = pieces - extra
    tiles, total = units // 128, places * main + over
    schedule = (0, 0, 1, 5, 7) if half == 4 else (0,) + (0,) * (half - 1) + (1,)
    dims = types.SimpleNamespace(
        places=places, columns=columns, width=width, main=main, over=over, pieces=pieces, direct=direct, tiles=tiles,
        schedule=schedule,
    )
    packed = STATE_ONE + STATE_TWO
    square = (blocks, 2, BLOCK, BLOCK)
    ring = columns - 1
    vmem = lambda *shape, dtype=bf16: pltpu.VMEM(shape, dtype)
    dma = lambda *shape: pltpu.SemaphoreType.DMA(shape)
    spaces = {"ref": pltpu.VMEM, "hbm": pl.ANY}
    in_specs = [
        pl.BlockSpec(memory_space=pltpu.SMEM if a.shape == (2, 2) else spaces[name[-3:]]) for name, a in given.items()
    ]
    lane_rows = PIECE // 128
    scratch = dict(
        value_in=vmem(2 * positions, BLOCK),
        gate_in=vmem(2 * positions, BLOCK),
        keys_in=vmem(positions, lanes),
        value_rim=vmem(16, BLOCK),
        keys_rim=vmem(16, lanes),
        value_wide=vmem(2 * positions + 16, BLOCK, dtype=f32),
        keys_wide=vmem(positions + 16, lanes, dtype=f32),
        gate_wide=vmem(2 * BLOCK, BLOCK, dtype=f32),
        conv_wide=vmem(2 * BLOCK, BLOCK, dtype=f32),
        x_s=vmem(*square),
        kt_s=vmem(*square),
        q_s=vmem(*square),
        state_s=vmem(*square, dtype=f32),
        near_s=vmem(*square, dtype=f32),
        stride_s=vmem(HEADS * blocks, BLOCK, dtype=f32),
        run_s=vmem(HEADS * blocks, BLOCK, dtype=f32),
        fade_s=vmem(HEADS * blocks, BLOCK, dtype=f32),
        end_s=vmem(HEADS * blocks, BLOCK, dtype=f32),
        cols_s=vmem(blocks, BLOCK, HEADS, dtype=f32),
        own_pack=vmem(packed, BLOCK),
        own_fade=vmem(8, BLOCK, dtype=f32),
        mate_pack=vmem(packed, BLOCK),
        mate_fade=vmem(8, BLOCK, dtype=f32),
        chip_pack=vmem(packed, BLOCK),
        chip_fade=vmem(8, BLOCK, dtype=f32),
        all_pack=vmem(chips, packed // 2, BLOCK),
        all_fade=vmem(chips, 8, BLOCK, dtype=f32),
        enter_pack=vmem(packed, BLOCK),
        carry_s=vmem(2, BLOCK, BLOCK, dtype=f32),
        mixed_s=vmem(columns, BLOCK, 2 * BLOCK),
        heads_in=vmem(columns, BLOCK, 2 * BLOCK),
        matrix=vmem(columns, 2 * BLOCK, width),
        acc_s=vmem(rows, width, dtype=f32),
        stream_s=vmem(rows, width),
        tables=vmem(columns, 8, rows, dtype=f32),
        put=vmem(columns, total, rows),
        pick=vmem(columns, 2, rows, total),
        share_s=vmem(columns, 2, rows, 128, dtype=f32),
        tokens=vmem(columns, extra, rows, PIECE),
        outbound=vmem(direct, places * main, PIECE),
        over_out=vmem(over, direct * lane_rows, 128, dtype=f32),
        over_in=vmem(over, direct * lane_rows, 128, dtype=f32),
        over_back=vmem(over, direct * lane_rows, 128, dtype=f32),
        over_ret=vmem(over, direct * lane_rows, 128, dtype=f32),
        over_total=vmem(direct, over, PIECE, dtype=f32),
        xout=vmem(columns, extra, places * main, PIECE),
        xback=vmem(columns, extra, places * main, PIECE),
        xret=vmem(columns, extra, total, PIECE),
        xover_out=vmem(columns, over, extra * lane_rows, 128, dtype=f32),
        xover_in=vmem(columns, over, extra * lane_rows, 128, dtype=f32),
        xover_back=vmem(columns, over, extra * lane_rows, 128, dtype=f32),
        xover_ret=vmem(columns, over, extra * lane_rows, 128, dtype=f32),
        chunks=vmem(columns, pieces, total, PIECE),
        hidden=vmem(columns, total, units),
        gate_up=vmem(tiles, width, 256),
        down=vmem(pieces, units, PIECE),
        sum_right=vmem(half + 1, direct, total, PIECE),
        sum_left=vmem(half + 1, direct, total, PIECE),
        xsum_right=vmem(half + 1, extra, rows, PIECE),
        xsum_left=vmem(half + 1, extra, rows, PIECE),
        totals=vmem(direct, places * main, PIECE),
        returned=vmem(direct, total, PIECE),
        load_sem=dma(5 + 2 * tiles + pieces),
    )
    for name, shape in dict(
        rim=(2,), mate=(2,), chip=(2, chips), enter=(1,), head=(columns,), table=(columns,), ring=(2, ring),
        over=(2,), token=(2, half, extra), out=(direct,), xout=(columns,), xover=(2, columns), chunk=(2, half, direct),
        xback=(columns,), sum=(2, half + 1, direct), xsum=(2, half + 1, extra), back=(direct,),
    ).items():
        scratch[name + "_send"], scratch[name + "_recv"] = dma(*shape), dma(*shape)
    scratch["pass_send"], scratch["pass_recv"] = dma(2, ring), dma(2, ring)
    names = [*given, "out_ref", *scratch]
    return pl.pallas_call(
        functools.partial(layer_kernel, dims, names),
        out_shape=jax.ShapeDtypeStruct((rows, width), bf16),
        in_specs=in_specs,
        out_specs=pl.BlockSpec(memory_space=pltpu.VMEM),
        scratch_shapes=list(scratch.values()),
        compiler_params=pltpu.CompilerParams(
            collective_id=0, has_side_effects=True, vmem_limit_bytes=VMEM_LIMIT
        ),
        name="layer",
    )(*given.values())


def local(
    residual,
    grouped_value_heads,
    output_gate_heads,
    projected_key_query,
    raw_step_size,
    step_size_bias,
    head_decay_logarithm,
    position_extra_decay,
    head_skip_weight,
    value_kernel_taps,
    key_query_kernel,
    head_norm_gain,
    output_matrix,
    expert_norm_gain,
    expert_gate_weight,
    expert_up_weight,
    expert_down_weight,
    token_expert_choice,
    expert_output_weight,
):
    return layer(
        lax.axis_size("sp"),
        lax.axis_size("tp"),
        residual_ref=residual,
        value_hbm=grouped_value_heads.reshape(-1, BLOCK),
        gate_hbm=output_gate_heads.reshape(-1, BLOCK),
        keys_hbm=projected_key_query,
        raw_ref=raw_step_size.transpose(1, 2, 0),
        bias_ref=step_size_bias,
        log_ref=head_decay_logarithm,
        extra_ref=position_extra_decay.reshape(-1, BLOCK),
        skip_ref=head_skip_weight,
        value_tap_ref=value_kernel_taps.reshape(-1, BLOCK),
        key_tap_ref=key_query_kernel,
        head_gain_ref=head_norm_gain,
        matrix_hbm=output_matrix,
        expert_gain_ref=expert_norm_gain[None],
        choice_ref=token_expert_choice.T,
        share_ref=expert_output_weight.T,
        expert_gate_hbm=expert_gate_weight,
        expert_up_hbm=expert_up_weight,
        expert_down_hbm=expert_down_weight,
    )


def solution(mesh):
    placed = (
        P(("grp", "sp", "tp"), None),
        P(("grp", "sp"), None, "tp"),
        P(("grp", "sp"), None, "tp"),
        P(("grp", "sp"), None),
        P(("grp", "sp"), None, "tp"),
        P(None, "tp"),
        P(None, "tp"),
        P(("grp", "sp")),
        P(None, "tp"),
        P(None, None, "tp"),
        P(),
        P(None, "tp"),
        P(None, "tp", None),
        P(),
        P("sp", None, "tp"),
        P("sp", None, "tp"),
        P("sp", "tp", None),
        P(("grp", "sp", "tp"), None),
        P(("grp", "sp", "tp"), None),
    )
    return jax.shard_map(
        local, mesh=mesh, in_specs=placed, out_specs=P(("grp", "sp", "tp"), None), check_vma=False
    )
```

profile of v0, /device:TPU:513, one launch (start us, length us, event | category | flops | bytes accessed | tf_op | source)
XLA Modules:
  0.0 257.8 jit_solution(7691985385643762566)
XLA Ops:
  0.0 255.9 %layer.1 = bf16[128,2048]{1,0:T(8,128)(2,1)} custom-call(bf16[128,2048]{1,0:T(8,128)(2,1)} %refs_0_.1, bf16[2048,128]{1,0:T(8,128)(2,1)} %bitcast.8, bf16[2048,128]{1,0:T(8,128)(2,1)} %bitcast.9, bf16[1024,384]{1,0:T(8,128)(2,1)} %refs_3_.1, bf16[2,2,1024]{2,1,0:T(2,128)(2,1)} %bitcast.10, f32[2,2]{1,0:T(2,128)} %refs_5_.1, f32[2,2]{1,0:T(2,128)} %refs_6_.1, ...), custom_call_target="tpu_custom_call" | custom-call | tf_op jit(solution)/shard_map/layer/pallas_call | solution.py:980
  255.9 1.9 copy.21
where the time goes:
time: 258 us
  Pallas kernels  256 us (99%)
    pallas_call x1, Pallas kernels, layer(): pl.pallas_call(functools.partial(layer_kernel, dims, names), out_shape=ja...  256 us

commit v1 on v0

--- a/solution.py
+++ b/solution.py
@@ -466,11 +466,6 @@
         for way in range(2):
             token_ring(way, 0, q, me_x).start()
 
-    for i in range(1, places):
-        remote(
-            r.over_out.at[place(i)], r.over_in.at[me_s], r.over_send.at[0], r.over_recv.at[0], {"sp": place(i)}
-        ).start()
-
     def send_out(p, carry):
         for i in range(1, places):
             remote(
@@ -484,6 +479,10 @@
         return carry
 
     lax.fori_loop(0, direct, send_out, 0)
+    for i in range(1, places):
+        remote(
+            r.over_out.at[place(i)], r.over_in.at[me_s], r.over_send.at[0], r.over_recv.at[0], {"sp": place(i)}
+        ).start()
     r.over_in[me_s] = r.over_out[me_s]
     if places < over:
         r.over_in[places:over] = jnp.zeros((over - places, *r.over_in.shape[1:]), f32)
@@ -561,8 +560,12 @@
         route(k)
 
     def chunk_ring(way, step, p, col):
-        here = r.chunks.at[col, p]
+        here = r.chunks.at[col, p, pl.ds(0, slots), :]
         return remote(here, here, r.chunk_send.at[way, step, p], r.chunk_recv.at[way, step, p], toward(way))
+
+    def over_ring(way, step, col):
+        here = r.chunks.at[col, pl.ds(0, direct), pl.ds(slots, over), :]
+        return remote(here, here, r.tail_send.at[way, step], r.tail_recv.at[way, step], toward(way))
 
     def out_arrived(p):
         most = pl.ds(0, (places - 1) * main)
@@ -575,17 +578,35 @@
         chunk_ring(0, 0, p, me_x).start()
         chunk_ring(1, 0, p, me_x).start()
 
-    remote(
-        r.over_out.at[0 : places - 1], r.over_in.at[0 : places - 1], r.over_send.at[0], r.over_recv.at[0], right
-    ).wait_recv()
-    for c in range(direct * lanes_of):
-        at_lanes = (c % lanes_of) * 128
-        r.chunks[me_x, c // lanes_of, slots:, at_lanes : at_lanes + 128] = r.over_in[:, c, :].astype(bf16)
-    for n in range(max(direct, half)):
-        if n < direct:
-            start_piece(n)
-        if n < half:
-            token_event(n + 1)
+    def start_over():
+        remote(
+            r.over_out.at[0 : places - 1], r.over_in.at[0 : places - 1], r.over_send.at[0], r.over_recv.at[0], right
+        ).wait_recv()
+        for c in range(direct * lanes_of):
+            at_lanes = (c % lanes_of) * 128
+            r.chunks[me_x, c // lanes_of, slots:, at_lanes : at_lanes + 128] = r.over_in[:, c, :].astype(bf16)
+        for way in range(2):
+            over_ring(way, 0, me_x).start()
+
+    for copy in rims + mates + [enter_copy]:
+        copy.wait_send()
+    for n in range(1, chips):
+        for which in range(2):
+            to_chip(n, which).wait_send()
+    for i in range(1, columns):
+        head_copy(column(i)).wait_send()
+        table_copy(i).wait_send()
+    for event in range(columns - 1):
+        for way in range(2):
+            matrix_ring(way, event, me_x).wait_send()
+            matrix_pass(way, event, me_x).wait_send()
+
+    for step in dims.opening:
+        if step > 0:
+            token_event(step)
+        elif -step < direct:
+            start_piece(-step)
+    start_over()
 
     def offset_of(n):
         k = lax.div(n + 1, 2)
@@ -662,9 +683,40 @@
 
         lax.fori_loop(low, high, body, 0)
 
+    def hop(way, j, p):
+        return remote(
+            r.sums.at[way, j, p],
+            r.sums.at[way, j - 1, p],
+            r.sum_send.at[way, j - 1, p],
+            r.sum_recv.at[way, j - 1, p],
+            {"tp": column(1 - 2 * way)},
+        )
+
+    def chains(long, step, group):
+        j = half - step if long else half - 1 - step
+
+        def body(p, carry):
+            odd = lax.rem(p, 2)
+            way = 1 - odd if long else odd
+            value = own(column(j * (1 - 2 * way)), p)
+            if step > 0:
+                hop(way, j + 1, p).wait_recv()
+                value = value + r.sums[way, j, p].astype(f32)
+            r.sums[way, j, p] = value.astype(bf16)
+            hop(way, j, p).start()
+            return carry
+
+        lax.fori_loop(*group, body, 0)
+
     share_of = dims.schedule
     for k in range(1, half + 1):
         first, last = share_of[k - 1] * dims.tiles, share_of[k] * dims.tiles
+
+        if k == half and half > 1:
+            units(first, last)
+            first = last
+            for group in dims.groups:
+                chains(False, 0, group)
 
         def pass_on(p, carry, k=k, first=first, last=last):
             for way in range(2):
@@ -687,47 +739,21 @@
             return carry
 
         lax.fori_loop(0, direct, pass_on, 0)
+        for way in range(2):
+            if k <= far(way, 0):
+                col = column(-k if way == 0 else k)
+                over_ring(way, k - 1, col).wait_recv()
+                if k < far(way, 0):
+                    over_ring(way, k, col).start()
         if k == 1:
             lax.fori_loop(0, columns, lambda col, carry: (make_pick(col), carry)[1], 0)
     units(share_of[half] * dims.tiles, columns * dims.tiles)
-
-    def hop(way, j, p):
-        buffer = r.sum_right if way == 0 else r.sum_left
-        return remote(
-            buffer.at[j, p],
-            buffer.at[j - 1, p],
-            r.sum_send.at[way, j - 1, p],
-            r.sum_recv.at[way, j - 1, p],
-            toward(way),
-        )
-
-    def round_of(t, low_piece, high_piece):
-        def body(p, carry):
-            for way in range(2):
-                buffer = r.sum_right if way == 0 else r.sum_left
-                j = far(1 - way, p) - t
-
-                def work(way=way, buffer=buffer, j=j):
-                    value = own(column(j if way == 0 else -j), p)
-                    if t > 0:
-                        hop(way, j + 1, p).wait_recv()
-                        value = value + buffer[j, p].astype(f32)
-                    buffer[j, p] = value.astype(bf16)
-                    hop(way, j, p).start()
-
-                if t < half - 1:
-                    work()
-                else:
-                    pl.when(j >= 1)(work)
-            return carry
-
-        lax.fori_loop(low_piece, high_piece, body, 0)
 
     def finish(p, carry):
         value = own(me_x, p)
         hop(0, 1, p).wait_recv()
         hop(1, 1, p).wait_recv()
-        value = value + r.sum_right[0, p].astype(f32) + r.sum_left[0, p].astype(f32)
+        value = value + r.sums[0, 0, p].astype(f32) + r.sums[1, 0, p].astype(f32)
         r.totals[p] = value[0:slots].astype(bf16)
         r.over_total[p] = value[slots:]
         r.returned[p, lines(me_s), :] = r.totals[p, lines(me_s), :]
@@ -788,13 +814,42 @@
                 buffer[j, q] = value.astype(bf16)
                 token_hop(way, j, q).start()
 
-    for t in range(half - 1):
-        round_of(t, 0, direct)
-    token_round(0)
-    round_of(half - 1, 0, direct)
-    if half > 1:
-        token_round(1)
-    lax.fori_loop(0, direct, finish, 0)
+    for group in dims.groups:
+        chains(True, 0, group)
+    remote(
+        r.over_out.at[0 : places - 1], r.over_in.at[0 : places - 1], r.over_send.at[0], r.over_recv.at[0], right
+    ).wait_send()
+    for way in range(2):
+        for q in range(extra):
+            for k in range(far(way, q)):
+                token_ring(way, k, q, me_x).wait_send()
+        for k in range(far(way, 0)):
+            over_ring(way, k, me_x).wait_send()
+
+    def drain_gather(p, carry):
+        out_arrived(p).wait_send()
+        for way in range(2):
+            for k in range(half):
+                pl.when(k < far(way, p))(lambda way=way, k=k: chunk_ring(way, k, p, me_x).wait_send())
+        return carry
+
+    lax.fori_loop(0, direct, drain_gather, 0)
+
+    def drain_routed(offset, carry):
+        for copy in routed(offset):
+            copy.wait_send()
+        return carry
+
+    lax.fori_loop(0, columns, drain_routed, 0)
+    for kind, step, group in dims.closing:
+        if kind == "short":
+            chains(False, step, group)
+        elif kind == "long":
+            chains(True, step, group)
+        elif kind == "token":
+            token_round(step)
+        else:
+            lax.fori_loop(*group, finish, 0)
     for c in range(direct * lanes_of):
         at_lanes = (c % lanes_of) * 128
         r.over_back[:, c, :] = r.over_total[c // lanes_of, :, at_lanes : at_lanes + 128]
@@ -803,8 +858,22 @@
         remote(
             r.over_back.at[place(i)], r.over_ret.at[me_s], r.over_send.at[1], r.over_recv.at[1], {"sp": place(i)}
         ).start()
-    for t in range(2, half):
-        token_round(t)
+
+    def drain_back(offset, carry):
+        for copy in given_back(offset):
+            copy.wait_send()
+        return carry
+
+    lax.fori_loop(0, columns, drain_back, 0)
+
+    def drain_sums(p, carry):
+        for way in range(2):
+            for k in range(half):
+                pl.when(k < far(1 - way, p))(lambda way=way, k=k: hop(way, k + 1, p).wait_send())
+        return carry
+
+    lax.fori_loop(0, direct, drain_sums, 0)
+    token_round(half - 1)
     take_back(0)
     for q in range(extra):
         value = weighted(me_x, r.xret.at[me_x], q)
@@ -836,45 +905,15 @@
 
     lax.fori_loop(0, direct, combine, 0)
 
-    for copy in rims + mates + [enter_copy]:
-        copy.wait_send()
-    for n in range(1, chips):
-        for which in range(2):
-            to_chip(n, which).wait_send()
-    for i in range(1, columns):
-        head_copy(column(i)).wait_send()
-        table_copy(i).wait_send()
-    for event in range(columns - 1):
-        for way in range(2):
-            matrix_ring(way, event, me_x).wait_send()
-            matrix_pass(way, event, me_x).wait_send()
-    for n, (a, b) in enumerate(((r.over_out, r.over_in), (r.over_back, r.over_ret))):
-        remote(a.at[0 : places - 1], b.at[0 : places - 1], r.over_send.at[n], r.over_recv.at[n], right).wait_send()
+    remote(
+        r.over_back.at[0 : places - 1], r.over_ret.at[0 : places - 1], r.over_send.at[1], r.over_recv.at[1], right
+    ).wait_send()
     for q in range(extra):
         for way in range(2):
-            for k in range(far(way, q)):
-                token_ring(way, k, q, me_x).wait_send()
             for k in range(far(1 - way, q)):
                 token_hop(way, k + 1, q).wait_send()
-
-    def drain_columns(offset, carry):
-        for copy in routed(offset) + given_back(offset):
-            copy.wait_send()
-        return carry
-
-    lax.fori_loop(0, columns, drain_columns, 0)
-
-    def drain(p, carry):
-        out_arrived(p).wait_send()
+    for p in range(direct):
         back_arrived(p).wait_send()
-        for way in range(2):
-            for k in range(half):
-                pl.when(k < far(way, p))(lambda way=way, k=k: chunk_ring(way, k, p, me_x).wait_send())
-                pl.when(k < far(1 - way, p))(lambda way=way, k=k: hop(way, k + 1, p).wait_send())
-        return carry
-
-    lax.fori_loop(0, direct, drain, 0)
-
 
 def layer(places, columns, **given):
     f32, bf16 = jnp.float32, jnp.bfloat16
@@ -889,10 +928,24 @@
     extra = max(1, pieces // 4)
     direct = pieces - extra
     tiles, total = units // 128, places * main + over
-    schedule = (0, 0, 1, 5, 7) if half == 4 else (0,) + (0,) * (half - 1) + (1,)
+    schedule = (0, 0, 1, 5, 7) if half == 4 else (0,) * half + (columns - 1,)
+    opening = (1, 0, 2, -1, -2, 3, -3, -4, 4, -5) if half == 4 else (*range(1, half + 1), *range(0, -direct, -1))
+    groups = [(low, min(low + 2, direct)) for low in range(0, direct, 2)]
+    closing = []
+    for n, group in enumerate(groups):
+        last = n == len(groups) - 1
+        for step in range(1, half):
+            if step < half - 1:
+                closing.append(("short", step, group))
+            closing.append(("long", step, group))
+            if last and step < half:
+                closing.append(("token", step - 1, None))
+        if n > 0:
+            closing.insert(len(closing) - half, ("finish", None, groups[n - 1]))
+    closing.append(("finish", None, groups[-1]))
     dims = types.SimpleNamespace(
         places=places, columns=columns, width=width, main=main, over=over, pieces=pieces, direct=direct, tiles=tiles,
-        schedule=schedule,
+        schedule=schedule, opening=opening, groups=groups, closing=closing,
     )
     packed = STATE_ONE + STATE_TWO
     square = (blocks, 2, BLOCK, BLOCK)
@@ -961,8 +1014,7 @@
         hidden=vmem(columns, total, units),
         gate_up=vmem(tiles, width, 256),
         down=vmem(pieces, units, PIECE),
-        sum_right=vmem(half + 1, direct, total, PIECE),
-        sum_left=vmem(half + 1, direct, total, PIECE),
+        sums=vmem(2, half + 1, direct, total, PIECE),
         xsum_right=vmem(half + 1, extra, rows, PIECE),
         xsum_left=vmem(half + 1, extra, rows, PIECE),
         totals=vmem(direct, places * main, PIECE),
@@ -972,7 +1024,7 @@
     for name, shape in dict(
         rim=(2,), mate=(2,), chip=(2, chips), enter=(1,), head=(columns,), table=(columns,), ring=(2, ring),
         over=(2,), token=(2, half, extra), out=(direct,), xout=(columns,), xover=(2, columns), chunk=(2, half, direct),
-        xback=(columns,), sum=(2, half + 1, direct), xsum=(2, half + 1, extra), back=(direct,),
+        xback=(columns,), sum=(2, half + 1, direct), xsum=(2, half + 1, extra), back=(direct,), tail=(2, half),
     ).items():
         scratch[name + "_send"], scratch[name + "_recv"] = dma(*shape), dma(*shape)
     scratch["pass_send"], scratch["pass_recv"] = dma(2, ring), dma(2, ring)

time: 258 us -> 247 us (0.957)
  Pallas kernels: 256 us -> 245 us
    pallas_call x1, Pallas kernels: 256 us -> 245 us  [layer(): pl.pallas_call(functools.partial(layer_kernel, dims, names), out_shape=ja...]
where the time goes in v1:
time: 247 us
  Pallas kernels  245 us (99%)
    pallas_call x1, Pallas kernels, layer(): pl.pallas_call(functools.partial(layer_kernel, dims, names), out_shape=ja...  245 us

profile of v1, /device:TPU:513, one launch (start us, length us, event | category | flops | bytes accessed | tf_op | source)
XLA Modules:
  0.0 247.2 jit_solution(8713027711244804797)
XLA Ops:
  0.0 245.4 %layer.1 = bf16[128,2048]{1,0:T(8,128)(2,1)} custom-call(bf16[128,2048]{1,0:T(8,128)(2,1)} %refs_0_.1, bf16[2048,128]{1,0:T(8,128)(2,1)} %bitcast.8, bf16[2048,128]{1,0:T(8,128)(2,1)} %bitcast.9, bf16[1024,384]{1,0:T(8,128)(2,1)} %refs_3_.1, bf16[2,2,1024]{2,1,0:T(2,128)(2,1)} %bitcast.10, f32[2,2]{1,0:T(2,128)} %refs_5_.1, f32[2,2]{1,0:T(2,128)} %refs_6_.1, ...), custom_call_target="tpu_custom_call" | custom-call | tf_op jit(solution)/shard_map/layer/pallas_call | solution.py:1032
  245.4 1.9 copy.21

commit v2 on v1

--- a/solution.py
+++ b/solution.py
@@ -17,6 +17,7 @@
 MESH = pl.DeviceIdType.MESH
 PIECE = 256
 HEADS = 4
+RING_SHARE = 6
 VMEM_LIMIT = 67043328
 
 
@@ -54,23 +55,33 @@
     def toward(way):
         return right if way == 0 else left
 
+    ring_part, slab = dims.ring_part, rows // chips
+    mine = pl.multiple_of(core * rows, rows)
+
+    def slab_rows(y):
+        return pl.ds(pl.multiple_of(mine + y * slab, 16), slab)
+
+    on_ring, on_grid = pl.ds(0, ring_part), pl.ds(ring_part, width - ring_part)
     loads = [
-        (r.matrix_hbm.at[0], r.matrix.at[me_x, pl.ds(0, rows), :]),
-        (r.matrix_hbm.at[1], r.matrix.at[me_x, pl.ds(rows, rows), :]),
+        (r.matrix_hbm.at[0], r.matrix.at[0, pl.ds(0, rows), :]),
+        (r.matrix_hbm.at[1], r.matrix.at[0, pl.ds(rows, rows), :]),
         (r.value_hbm, r.value_in),
         (r.keys_hbm, r.keys_in),
         (r.gate_hbm, r.gate_in),
     ]
-    early = len(loads)
-    for t in range(dims.tiles):
-        span = pl.ds(t * 128, 128)
-        loads.append((r.expert_gate_hbm.at[0, :, span], r.gate_up.at[t, :, pl.ds(0, 128)]))
-        loads.append((r.expert_up_hbm.at[0, :, span], r.gate_up.at[t, :, pl.ds(128, 128)]))
-    for p in range(dims.pieces):
-        loads.append((r.expert_down_hbm.at[0, :, pl.ds(p * PIECE, PIECE)], r.down.at[p]))
     loads = [pltpu.make_async_copy(a, b, r.load_sem.at[n]) for n, (a, b) in enumerate(loads)]
     for load in loads:
         load.start()
+    for t in range(dims.tiles):
+        span = pl.ds(t * 128, 128)
+        for n, weight in enumerate((r.expert_gate_hbm, r.expert_up_hbm)):
+            pltpu.make_async_copy(
+                weight.at[0, :, span], r.gate_up.at[t, :, pl.ds(n * 128, 128)], r.weight_sem.at[0]
+            ).start()
+    for p in range(dims.pieces):
+        pltpu.make_async_copy(
+            r.expert_down_hbm.at[0, :, pl.ds(p * PIECE, PIECE)], r.down.at[p], r.weight_sem.at[1]
+        ).start()
 
     barrier = pltpu.get_barrier_semaphore()
     peers = [{"tp": column(i)} for i in range(1, columns)] + [{"sp": place(i)} for i in range(1, places)]
@@ -122,20 +133,52 @@
     r.tables[me_x, 0:2, :] = r.choice_ref[...].astype(f32)
     r.tables[me_x, 2:4, :] = r.share_ref[...]
 
-    for load in loads[: early - 1]:
+    for load in loads[:-1]:
         load.wait()
     pl.semaphore_wait(barrier, len(peers))
 
-    cut = width // 2
-    mine = pl.ds(pl.multiple_of(core * rows, rows), rows)
-
-    def matrix_ring(way, event, col):
-        here = r.matrix.at[col, mine, pl.ds(((event % 2) ^ way) * cut, cut)]
-        return remote(here, here, r.ring_send.at[way, event], r.ring_recv.at[way, event], toward(way))
-
-    def matrix_pass(way, event, col):
-        here = r.matrix.at[col, mine, pl.ds(((event % 2) ^ way) * cut, cut)]
-        return remote(here, here, r.pass_send.at[way, event], r.pass_recv.at[way, event], mate)
+    def matrix_block(way, event, k):
+        piece = (event % 2) ^ way
+        block = (columns - k if way == 0 else k) % columns
+        return r.matrix.at[block, pl.ds(pl.multiple_of(mine + piece * (rows // 2), 16), rows // 2), on_ring]
+
+    def matrix_ring(way, event):
+        k = event // 2
+        return remote(
+            matrix_block(way, event, k),
+            matrix_block(way, event, k + 1),
+            r.ring_send.at[0],
+            r.ring_recv.at[way, event],
+            toward(way),
+        )
+
+    def slab_copy(offset):
+        return remote(
+            r.matrix.at[0, slab_rows(me_y), on_grid],
+            r.matrix.at[columns - offset, slab_rows(me_y), on_grid],
+            r.slab_send.at[0],
+            r.slab_recv.at[0],
+            {"tp": column(offset)},
+        )
+
+    def grid_view(way, event, y):
+        blocks_of = pl.ds(1, half) if (event % 2) ^ way == 0 else pl.ds(1 + half, half - 1)
+        return r.matrix.at[blocks_of, slab_rows(y), on_grid]
+
+    def grid_ring(way, event, y):
+        here = grid_view(way, event, y)
+        return remote(
+            here, here, r.grid_send.at[0], r.grid_recv.at[way, event], peer(1) if way == 0 else peer(chips - 1)
+        )
+
+    def to_mate(here, which):
+        return remote(here, here, r.pass_send.at[which], r.pass_recv.at[which], mate)
+
+    most_columns, other_blocks = pl.ds(0, columns - 1), pl.ds(1, columns - 1)
+    ring_total = r.matrix.at[other_blocks, pl.ds(0, rows), on_ring]
+    grid_total = r.matrix.at[other_blocks, pl.ds(0, (chips - 1) * slab), on_grid]
+    slab_total = r.matrix.at[other_blocks, pl.ds(0, slab), on_grid]
+    pass_totals = (ring_total, r.matrix.at[other_blocks, pl.ds(0, rows), on_grid])
 
     rim_rows = 16
     positions = blocks * rows
@@ -155,29 +198,52 @@
         rim.start()
 
     def table_copy(offset):
-        return remote(
-            r.tables.at[me_x],
-            r.tables.at[me_x],
-            r.table_send.at[offset],
-            r.table_recv.at[columns - offset],
-            {"tp": column(offset)},
-        )
+        here = r.tables.at[me_x]
+        return remote(here, here, r.table_send.at[0], r.table_recv.at[0], {"tp": column(offset)})
 
     for i in range(1, columns):
         table_copy(i).start()
+    for i in range(1, columns):
+        slab_copy(i).start()
     for event in range(2):
         for way in range(2):
             if event < columns - 1:
-                matrix_ring(way, event, me_x).start()
-
-    def service(event):
+                matrix_ring(way, event).start()
+    tables_total = remote(
+        r.tables.at[most_columns], r.tables.at[most_columns], r.table_send.at[0], r.table_recv.at[0], right
+    )
+
+    def serve_ring(event):
+        for way in range(2):
+            matrix_ring(way, event).wait_recv()
+            if event + 2 < columns - 1:
+                matrix_ring(way, event + 2).start()
+            to_mate(matrix_block(way, event, event // 2 + 1), 0).start()
+
+    def serve_slab():
+        remote(slab_total, slab_total, r.slab_send.at[0], r.slab_recv.at[0], right).wait_recv()
+        for event in range(2):
+            for way in range(2):
+                if event < chips - 1:
+                    grid_ring(way, event, me_y).start()
+        to_mate(r.matrix.at[other_blocks, slab_rows(me_y), on_grid], 1).start()
+
+    def serve_grid(event):
         k = event // 2 + 1
         for way in range(2):
-            col = column(-k if way == 0 else k)
-            matrix_ring(way, event, col).wait_recv()
-            if event + 2 < columns - 1:
-                matrix_ring(way, event + 2, col).start()
-            matrix_pass(way, event, col).start()
+            y = lax.rem(me_y + (chips - k if way == 0 else k), chips)
+            grid_ring(way, event, y).wait_recv()
+            if event + 2 < chips - 1:
+                grid_ring(way, event + 2, y).start()
+            to_mate(grid_view(way, event, y), 1).start()
+
+    waiting = [("x", e) for e in range(columns - 1)] + [("y", e) for e in range(chips - 1)]
+
+    def serve(*steps):
+        for step in steps:
+            if step in waiting:
+                waiting.remove(step)
+                (serve_ring if step[0] == "x" else serve_grid)(step[1])
 
     r.value_wide[rim_rows:, :] = r.value_in[...].astype(f32)
     r.keys_wide[rim_rows:, :] = r.keys_in[...].astype(f32)
@@ -252,7 +318,6 @@
     ]
     for copy in mates:
         copy.start()
-    service(0)
     for copy in mates:
         copy.wait_recv()
     is_low = core == 0
@@ -272,8 +337,12 @@
         return remote(src, dst, r.chip_send.at[which, n], r.chip_recv.at[which, n], peer(n))
 
     for n in range(1, chips):
-        for which in range(2):
-            to_chip(n, which).start()
+
+        @pl.when(me_y + n < chips)
+        def _():
+            for which in range(2):
+                to_chip(n, which).start()
+
 
     below = at_row >= at_lane
 
@@ -292,13 +361,48 @@
         return carry
 
     lax.fori_loop(0, blocks, near_step, 0)
-    if columns > 2:
-        service(1)
-    loads[early - 1].wait()
-
+    serve_slab()
+    serve(*dims.serving[0])
+    main, over, slots = dims.main, dims.over, places * dims.main
+    total_slots = slots + over
+    slot_row = lax.broadcasted_iota(jnp.int32, (total_slots, over), 0)
+    slot_expert = lax.broadcasted_iota(jnp.int32, (total_slots, over), 1)
+    spread = jnp.where(
+        ((slot_row < slots) & (slot_row >= slot_expert * main) & (slot_row < slot_expert * main + main))
+        | (slot_row == slots + slot_expert),
+        1.0,
+        0.0,
+    ).astype(bf16)
+    at = lax.broadcasted_iota(jnp.int32, (total_slots, rows), 0)
+    turn = jnp.where(at < slots, jnp.bitwise_and(at, main - 1), main).astype(f32)
+    expert_at = lax.broadcasted_iota(jnp.int32, (over, rows), 0).astype(f32)
+    earlier = jnp.where(at_row < at_lane, 1.0, 0.0).astype(bf16)
+
+    def make_put(col):
+        table = r.tables[col]
+        named = jnp.where((expert_at == table[0:1]) | (expert_at == table[1:2]), 1.0, 0.0)
+        rank = jnp.dot(named.astype(bf16), earlier, preferred_element_type=f32)
+        named_x = jnp.dot(spread, named.astype(bf16), preferred_element_type=f32)
+        rank_x = jnp.dot(spread, rank.astype(bf16), preferred_element_type=f32)
+        r.put[col] = jnp.where(rank_x == turn, named_x, 0.0).astype(bf16)
+
+    tables_total.wait_recv()
+
+    def put_step(col, carry):
+        make_put(col)
+        return carry
+
+    lax.fori_loop(0, columns, put_step, 0)
+
+    loads[-1].wait()
+    serve(*dims.serving[1])
     for n in range(1, chips):
-        for which in range(2):
-            to_chip(n, which).wait_recv()
+
+        @pl.when(me_y >= n)
+        def _():
+            for which in range(2):
+                to_chip(n, which).wait_recv()
+
     row_at = lax.broadcasted_iota(jnp.int32, (piece, rows), 0) + core * piece
     half_two = row_at < STATE_TWO
     entering = jnp.zeros((piece, rows), f32)
@@ -318,8 +422,9 @@
     r.carry_s[0] = jnp.zeros((rows, rows), f32)
     r.carry_s[0, 0:STATE_ONE, :] = entered[STATE_TWO:]
 
+    serve(*dims.serving[2])
     def head_copy(col):
-        return remote(r.mixed_s.at[col], r.heads_in.at[me_x], r.head_send.at[col], r.head_recv.at[me_x], {"tp": col})
+        return remote(r.mixed_s.at[col], r.heads_in.at[me_x], r.head_send.at[0], r.head_recv.at[0], {"tp": col})
 
     def mix_step(k, carry):
         cols = jnp.exp(r.cols_s[k])
@@ -354,38 +459,6 @@
     lax.fori_loop(0, blocks, mix_step, 0)
     r.heads_in[me_x] = r.mixed_s[me_x]
 
-    main, over, slots = dims.main, dims.over, places * dims.main
-    total_slots = slots + over
-    slot_row = lax.broadcasted_iota(jnp.int32, (total_slots, over), 0)
-    slot_expert = lax.broadcasted_iota(jnp.int32, (total_slots, over), 1)
-    spread = jnp.where(
-        ((slot_row < slots) & (slot_row >= slot_expert * main) & (slot_row < slot_expert * main + main))
-        | (slot_row == slots + slot_expert),
-        1.0,
-        0.0,
-    ).astype(bf16)
-    at = lax.broadcasted_iota(jnp.int32, (total_slots, rows), 0)
-    turn = jnp.where(at < slots, jnp.bitwise_and(at, main - 1), main).astype(f32)
-    expert_at = lax.broadcasted_iota(jnp.int32, (over, rows), 0).astype(f32)
-    earlier = jnp.where(at_row < at_lane, 1.0, 0.0).astype(bf16)
-
-    def make_put(col):
-        table = r.tables[col]
-        named = jnp.where((expert_at == table[0:1]) | (expert_at == table[1:2]), 1.0, 0.0)
-        rank = jnp.dot(named.astype(bf16), earlier, preferred_element_type=f32)
-        named_x = jnp.dot(spread, named.astype(bf16), preferred_element_type=f32)
-        rank_x = jnp.dot(spread, rank.astype(bf16), preferred_element_type=f32)
-        r.put[col] = jnp.where(rank_x == turn, named_x, 0.0).astype(bf16)
-
-    for i in range(1, columns):
-        table_copy(i).wait_recv()
-
-    def put_step(col, carry):
-        make_put(col)
-        return carry
-
-    lax.fori_loop(0, columns, put_step, 0)
-
     slot_col = lax.broadcasted_iota(jnp.int32, (over, total_slots), 1)
     slot_exp = lax.broadcasted_iota(jnp.int32, (over, total_slots), 0)
     spread_t = jnp.where(
@@ -409,28 +482,22 @@
             r.pick[col, k] = jnp.where(rank_x == turn_t, named_x, 0.0).astype(bf16)
             r.share_s[col, k] = jnp.broadcast_to(table[:, 2 + k : 3 + k], (rows, rows))
 
-    def arrived(col):
-        return remote(r.mixed_s.at[col], r.heads_in.at[col], r.head_send.at[col], r.head_recv.at[col], {"tp": col})
-
-    def product(col, first=False):
+    def product(block, first):
         for n in range(0, width, 512):
-            part = jnp.dot(r.heads_in[col], r.matrix[col, :, n : n + 512], preferred_element_type=f32)
-            r.acc_s[:, n : n + 512] = part if first else r.acc_s[:, n : n + 512] + part
-
-    product(me_x, True)
-    for event in range(2, columns - 1):
-        service(event)
-    for k in range(1, half + 1):
-        for way in range(2):
-            if way == 1 and k == half:
-                continue
-            for event in (2 * k - 2, 2 * k - 1):
-                if event < columns - 1:
-                    for side in range(2) if k == half else (way,):
-                        matrix_pass(side, event, column(k if side else -k)).wait_recv()
-            col = column(-k if way == 0 else k)
-            arrived(col).wait_recv()
-            product(col)
+            span = slice(n, n + 512)
+            part = jnp.dot(r.heads_in[column(block)], r.matrix[block, :, span], preferred_element_type=f32)
+            r.acc_s[:, span] = part if first else r.acc_s[:, span] + part
+
+    serve(*dims.serving[3])
+    serve(*list(waiting))
+    heads_total = remote(
+        r.mixed_s.at[most_columns], r.heads_in.at[most_columns], r.head_send.at[0], r.head_recv.at[0], right
+    )
+    heads_total.wait_recv()
+    remote(pass_totals[0], pass_totals[0], r.pass_send.at[0], r.pass_recv.at[0], mate).wait_recv()
+    remote(pass_totals[1], pass_totals[1], r.pass_send.at[1], r.pass_recv.at[1], mate).wait_recv()
+    for block in range(columns):
+        product(block, block == 0)
 
     stream = (r.residual_ref[...].astype(f32) + r.acc_s[...]).astype(bf16)
     r.stream_s[...] = stream
@@ -454,7 +521,7 @@
 
     def token_ring(way, step, q, col):
         here = r.tokens.at[col, q]
-        return remote(here, here, r.token_send.at[way, step, q], r.token_recv.at[way, step, q], toward(way))
+        return remote(here, here, r.token_send.at[0], r.token_recv.at[way, step, q], toward(way))
 
     put_own = r.put[me_x]
     for p in range(direct):
@@ -471,7 +538,7 @@
             remote(
                 r.outbound.at[p, lines(place(i)), :],
                 r.chunks.at[me_x, p, lines(me_s), :],
-                r.out_send.at[p],
+                r.out_send.at[0],
                 r.out_recv.at[p],
                 {"sp": place(i)},
             ).start()
@@ -503,14 +570,14 @@
             remote(
                 r.xout.at[col, :, lines(place(i)), :],
                 r.chunks.at[col, pl.ds(direct, extra), lines(me_s), :],
-                r.xout_send.at[offset],
+                r.xout_send.at[0],
                 r.xout_recv.at[offset],
                 {"sp": place(i)},
             ).start()
             remote(
                 r.xover_out.at[offset, place(i)],
                 r.xover_in.at[offset, me_s],
-                r.xover_send.at[0, offset],
+                r.xover_send.at[0],
                 r.xover_recv.at[0, offset],
                 {"sp": place(i)},
             ).start()
@@ -522,14 +589,14 @@
             remote(
                 r.xout.at[col, :, most, :],
                 r.chunks.at[col, pl.ds(direct, extra), most, :],
-                r.xout_send.at[offset],
+                r.xout_send.at[0],
                 r.xout_recv.at[offset],
                 right,
             ),
             remote(
                 r.xover_out.at[offset, 0 : places - 1],
                 r.xover_in.at[offset, 0 : places - 1],
-                r.xover_send.at[0, offset],
+                r.xover_send.at[0],
                 r.xover_recv.at[0, offset],
                 right,
             ),
@@ -561,16 +628,16 @@
 
     def chunk_ring(way, step, p, col):
         here = r.chunks.at[col, p, pl.ds(0, slots), :]
-        return remote(here, here, r.chunk_send.at[way, step, p], r.chunk_recv.at[way, step, p], toward(way))
+        return remote(here, here, r.chunk_send.at[0], r.chunk_recv.at[way, step, p], toward(way))
 
     def over_ring(way, step, col):
         here = r.chunks.at[col, pl.ds(0, direct), pl.ds(slots, over), :]
-        return remote(here, here, r.tail_send.at[way, step], r.tail_recv.at[way, step], toward(way))
+        return remote(here, here, r.tail_send.at[0], r.tail_recv.at[way, step], toward(way))
 
     def out_arrived(p):
         most = pl.ds(0, (places - 1) * main)
         return remote(
-            r.outbound.at[p, most, :], r.chunks.at[me_x, p, most, :], r.out_send.at[p], r.out_recv.at[p], right
+            r.outbound.at[p, most, :], r.chunks.at[me_x, p, most, :], r.out_send.at[0], r.out_recv.at[p], right
         )
 
     def start_piece(p):
@@ -591,15 +658,20 @@
     for copy in rims + mates + [enter_copy]:
         copy.wait_send()
     for n in range(1, chips):
-        for which in range(2):
-            to_chip(n, which).wait_send()
-    for i in range(1, columns):
-        head_copy(column(i)).wait_send()
-        table_copy(i).wait_send()
-    for event in range(columns - 1):
-        for way in range(2):
-            matrix_ring(way, event, me_x).wait_send()
-            matrix_pass(way, event, me_x).wait_send()
+
+        @pl.when(me_y + n < chips)
+        def _():
+            for which in range(2):
+                to_chip(n, which).wait_send()
+
+    heads_total.wait_send()
+    tables_total.wait_send()
+    remote(ring_total, ring_total, r.ring_send.at[0], r.ring_recv.at[0, 0], right).wait_send()
+    remote(slab_total, slab_total, r.slab_send.at[0], r.slab_recv.at[0], right).wait_send()
+    remote(grid_total, grid_total, r.grid_send.at[0], r.grid_recv.at[0, 0], right).wait_send()
+    for which in range(2):
+        view = pass_totals[which]
+        remote(view, view, r.pass_send.at[which], r.pass_recv.at[which], mate).wait_send()
 
     for step in dims.opening:
         if step > 0:
@@ -641,14 +713,14 @@
             remote(
                 r.xback.at[col, :, lines(place(i)), :],
                 r.xret.at[col, :, lines(me_s), :],
-                r.xback_send.at[offset],
+                r.xback_send.at[0],
                 r.xback_recv.at[offset],
                 {"sp": place(i)},
             ).start()
             remote(
                 r.xover_back.at[offset, place(i)],
                 r.xover_ret.at[offset, me_s],
-                r.xover_send.at[1, offset],
+                r.xover_send.at[1],
                 r.xover_recv.at[1, offset],
                 {"sp": place(i)},
             ).start()
@@ -660,21 +732,21 @@
             remote(
                 r.xback.at[col, :, most, :],
                 r.xret.at[col, :, most, :],
-                r.xback_send.at[offset],
+                r.xback_send.at[0],
                 r.xback_recv.at[offset],
                 right,
             ),
             remote(
                 r.xover_back.at[offset, 0 : places - 1],
                 r.xover_ret.at[offset, 0 : places - 1],
-                r.xover_send.at[1, offset],
+                r.xover_send.at[1],
                 r.xover_recv.at[1, offset],
                 right,
             ),
         )
 
-    for load in loads[early:]:
-        load.wait()
+    for n, weights in enumerate((r.gate_up, r.down)):
+        pltpu.make_async_copy(weights, weights, r.weight_sem.at[n]).wait()
 
     def units(low, high):
         def body(v, carry):
@@ -687,7 +759,7 @@
         return remote(
             r.sums.at[way, j, p],
             r.sums.at[way, j - 1, p],
-            r.sum_send.at[way, j - 1, p],
+            r.sum_send.at[0],
             r.sum_recv.at[way, j - 1, p],
             {"tp": column(1 - 2 * way)},
         )
@@ -761,7 +833,7 @@
             remote(
                 r.totals.at[p, lines(place(i)), :],
                 r.returned.at[p, lines(me_s), :],
-                r.back_send.at[p],
+                r.back_send.at[0],
                 r.back_recv.at[p],
                 {"sp": place(i)},
             ).start()
@@ -788,7 +860,7 @@
         return remote(
             buffer.at[j, q],
             buffer.at[j - 1, q],
-            r.xsum_send.at[way, j - 1, q],
+            r.xsum_send.at[0],
             r.xsum_recv.at[way, j - 1, q],
             toward(way),
         )
@@ -816,31 +888,18 @@
 
     for group in dims.groups:
         chains(True, 0, group)
-    remote(
-        r.over_out.at[0 : places - 1], r.over_in.at[0 : places - 1], r.over_send.at[0], r.over_recv.at[0], right
-    ).wait_send()
-    for way in range(2):
-        for q in range(extra):
-            for k in range(far(way, q)):
-                token_ring(way, k, q, me_x).wait_send()
-        for k in range(far(way, 0)):
-            over_ring(way, k, me_x).wait_send()
-
-    def drain_gather(p, carry):
-        out_arrived(p).wait_send()
-        for way in range(2):
-            for k in range(half):
-                pl.when(k < far(way, p))(lambda way=way, k=k: chunk_ring(way, k, p, me_x).wait_send())
-        return carry
-
-    lax.fori_loop(0, direct, drain_gather, 0)
-
-    def drain_routed(offset, carry):
-        for copy in routed(offset):
-            copy.wait_send()
-        return carry
-
-    lax.fori_loop(0, columns, drain_routed, 0)
+    def left_by_now(view, send, recv):
+        remote(view, view, send, recv, right).wait_send()
+
+    most_places, most_lines = pl.ds(0, places - 1), pl.ds(0, (places - 1) * main)
+    chunks_total = r.chunks.at[most_columns, pl.ds(0, direct), pl.ds(0, slots), :]
+    left_by_now(r.over_out.at[most_places], r.over_send.at[0], r.over_recv.at[0])
+    left_by_now(r.tokens.at[most_columns], r.token_send.at[0], r.token_recv.at[0, 0, 0])
+    left_by_now(r.chunks.at[most_columns, pl.ds(0, direct), pl.ds(slots, over), :], r.tail_send.at[0], r.tail_recv.at[0, 0])
+    left_by_now(chunks_total, r.chunk_send.at[0], r.chunk_recv.at[0, 0, 0])
+    left_by_now(r.outbound.at[:, most_lines, :], r.out_send.at[0], r.out_recv.at[0])
+    left_by_now(r.xout.at[:, :, most_lines, :], r.xout_send.at[0], r.xout_recv.at[0])
+    left_by_now(r.xover_out.at[:, most_places], r.xover_send.at[0], r.xover_recv.at[0, 0])
     for kind, step, group in dims.closing:
         if kind == "short":
             chains(False, step, group)
@@ -859,20 +918,9 @@
             r.over_back.at[place(i)], r.over_ret.at[me_s], r.over_send.at[1], r.over_recv.at[1], {"sp": place(i)}
         ).start()
 
-    def drain_back(offset, carry):
-        for copy in given_back(offset):
-            copy.wait_send()
-        return carry
-
-    lax.fori_loop(0, columns, drain_back, 0)
-
-    def drain_sums(p, carry):
-        for way in range(2):
-            for k in range(half):
-                pl.when(k < far(1 - way, p))(lambda way=way, k=k: hop(way, k + 1, p).wait_send())
-        return carry
-
-    lax.fori_loop(0, direct, drain_sums, 0)
+    left_by_now(r.xback.at[:, :, most_lines, :], r.xback_send.at[0], r.xback_recv.at[0])
+    left_by_now(r.xover_back.at[:, most_places], r.xover_send.at[1], r.xover_recv.at[1, 0])
+    left_by_now(r.chunks.at[most_columns, pl.ds(0, direct)], r.sum_send.at[0], r.sum_recv.at[0, 0, 0])
     token_round(half - 1)
     take_back(0)
     for q in range(extra):
@@ -893,7 +941,7 @@
     def back_arrived(p):
         most = pl.ds(0, (places - 1) * main)
         return remote(
-            r.totals.at[p, most, :], r.returned.at[p, most, :], r.back_send.at[p], r.back_recv.at[p], right
+            r.totals.at[p, most, :], r.returned.at[p, most, :], r.back_send.at[0], r.back_recv.at[p], right
         )
 
     def combine(p, carry):
@@ -905,15 +953,10 @@
 
     lax.fori_loop(0, direct, combine, 0)
 
-    remote(
-        r.over_back.at[0 : places - 1], r.over_ret.at[0 : places - 1], r.over_send.at[1], r.over_recv.at[1], right
-    ).wait_send()
-    for q in range(extra):
-        for way in range(2):
-            for k in range(far(1 - way, q)):
-                token_hop(way, k + 1, q).wait_send()
-    for p in range(direct):
-        back_arrived(p).wait_send()
+    left_by_now(r.over_back.at[most_places], r.over_send.at[1], r.over_recv.at[1])
+    left_by_now(r.tokens.at[most_columns], r.xsum_send.at[0], r.xsum_recv.at[0, 0, 0])
+    left_by_now(r.totals.at[:, most_lines, :], r.back_send.at[0], r.back_recv.at[0])
+
 
 def layer(places, columns, **given):
     f32, bf16 = jnp.float32, jnp.bfloat16
@@ -928,8 +971,15 @@
     extra = max(1, pieces // 4)
     direct = pieces - extra
     tiles, total = units // 128, places * main + over
+    ring_part = width * RING_SHARE // 16 // 128 * 128
     schedule = (0, 0, 1, 5, 7) if half == 4 else (0,) * half + (columns - 1,)
     opening = (1, 0, 2, -1, -2, 3, -3, -4, 4, -5) if half == 4 else (*range(1, half + 1), *range(0, -direct, -1))
+    serving = [
+        [("x", 0)],
+        [("x", 1), ("y", 0)],
+        [("x", 2), ("y", 1)],
+        [("x", 3), ("y", 2), ("x", 4), ("y", 3), ("y", 4), ("y", 5), ("x", 5), ("x", 6), ("y", 6)],
+    ]
     groups = [(low, min(low + 2, direct)) for low in range(0, direct, 2)]
     closing = []
     for n, group in enumerate(groups):
@@ -945,11 +995,10 @@
     closing.append(("finish", None, groups[-1]))
     dims = types.SimpleNamespace(
         places=places, columns=columns, width=width, main=main, over=over, pieces=pieces, direct=direct, tiles=tiles,
-        schedule=schedule, opening=opening, groups=groups, closing=closing,
+        schedule=schedule, opening=opening, groups=groups, closing=closing, ring_part=ring_part, serving=serving,
     )
     packed = STATE_ONE + STATE_TWO
     square = (blocks, 2, BLOCK, BLOCK)
-    ring = columns - 1
     vmem = lambda *shape, dtype=bf16: pltpu.VMEM(shape, dtype)
     dma = lambda *shape: pltpu.SemaphoreType.DMA(shape)
     spaces = {"ref": pltpu.VMEM, "hbm": pl.ANY}
@@ -1019,15 +1068,34 @@
         xsum_left=vmem(half + 1, extra, rows, PIECE),
         totals=vmem(direct, places * main, PIECE),
         returned=vmem(direct, total, PIECE),
-        load_sem=dma(5 + 2 * tiles + pieces),
+        load_sem=dma(5),
+        weight_sem=dma(2),
     )
-    for name, shape in dict(
-        rim=(2,), mate=(2,), chip=(2, chips), enter=(1,), head=(columns,), table=(columns,), ring=(2, ring),
-        over=(2,), token=(2, half, extra), out=(direct,), xout=(columns,), xover=(2, columns), chunk=(2, half, direct),
-        xback=(columns,), sum=(2, half + 1, direct), xsum=(2, half + 1, extra), back=(direct,), tail=(2, half),
-    ).items():
-        scratch[name + "_send"], scratch[name + "_recv"] = dma(*shape), dma(*shape)
-    scratch["pass_send"], scratch["pass_recv"] = dma(2, ring), dma(2, ring)
+    steps = (2, half)
+    for name, send, recv in (
+        ("rim", (2,), (2,)),
+        ("mate", (2,), (2,)),
+        ("chip", (2, chips), (2, chips)),
+        ("enter", (1,), (1,)),
+        ("head", (1,), (1,)),
+        ("table", (1,), (1,)),
+        ("ring", (1,), (2, columns - 1)),
+        ("slab", (1,), (1,)),
+        ("grid", (1,), (2, chips - 1)),
+        ("pass", (2,), (2,)),
+        ("over", (2,), (2,)),
+        ("token", (1,), (*steps, extra)),
+        ("out", (1,), (direct,)),
+        ("xout", (1,), (columns,)),
+        ("xover", (2,), (2, columns)),
+        ("chunk", (1,), (*steps, direct)),
+        ("tail", (1,), steps),
+        ("xback", (1,), (columns,)),
+        ("sum", (1,), (*steps, direct)),
+        ("xsum", (1,), (*steps, extra)),
+        ("back", (1,), (direct,)),
+    ):
+        scratch[name + "_send"], scratch[name + "_recv"] = dma(*send), dma(*recv)
     names = [*given, "out_ref", *scratch]
     return pl.pallas_call(
         functools.partial(layer_kernel, dims, names),

time: 247 us -> 230 us (0.931)
  Pallas kernels: 245 us -> 228 us
    pallas_call x1, Pallas kernels: 245 us -> 228 us  [layer(): pl.pallas_call(functools.partial(layer_kernel, dims, names), out_shape=ja...]
where the time goes in v2:
time: 230 us
  Pallas kernels  228 us (99%)
    pallas_call x1, Pallas kernels, layer(): pl.pallas_call(functools.partial(layer_kernel, dims, names), out_shape=ja...  228 us

profile of v2, /device:TPU:513, one launch (start us, length us, event | category | flops | bytes accessed | tf_op | source)
XLA Modules:
  0.0 229.9 jit_solution(5960651351362146196)
XLA Ops:
  0.0 228.0 %layer.1 = bf16[128,2048]{1,0:T(8,128)(2,1)} custom-call(bf16[128,2048]{1,0:T(8,128)(2,1)} %refs_0_.1, bf16[2048,128]{1,0:T(8,128)(2,1)} %bitcast.8, bf16[2048,128]{1,0:T(8,128)(2,1)} %bitcast.9, bf16[1024,384]{1,0:T(8,128)(2,1)} %refs_3_.1, bf16[2,2,1024]{2,1,0:T(2,128)(2,1)} %bitcast.10, f32[2,2]{1,0:T(2,128)} %refs_5_.1, f32[2,2]{1,0:T(2,128)} %refs_6_.1, ...), custom_call_target="tpu_custom_call" | custom-call | tf_op jit(solution)/shard_map/layer/pallas_call | solution.py:1100
  228.0 1.9 copy.21

commit v3 on v2

--- a/solution.py
+++ b/solution.py
@@ -17,7 +17,7 @@
 MESH = pl.DeviceIdType.MESH
 PIECE = 256
 HEADS = 4
-RING_SHARE = 6
+RING_SHARE = 7
 VMEM_LIMIT = 67043328
 
 
@@ -55,6 +55,11 @@
     def toward(way):
         return right if way == 0 else left
 
+    barrier = pltpu.get_barrier_semaphore()
+    peers = [{"tp": column(i)} for i in range(1, columns)] + [{"sp": place(i)} for i in range(1, places)]
+    for device in peers:
+        pl.semaphore_signal(barrier, inc=1, device_id=device, device_id_type=MESH)
+
     ring_part, slab = dims.ring_part, rows // chips
     mine = pl.multiple_of(core * rows, rows)
 
@@ -68,10 +73,128 @@
         (r.value_hbm, r.value_in),
         (r.keys_hbm, r.keys_in),
         (r.gate_hbm, r.gate_in),
+        (r.residual_hbm, r.residual_in),
     ]
     loads = [pltpu.make_async_copy(a, b, r.load_sem.at[n]) for n, (a, b) in enumerate(loads)]
     for load in loads:
         load.start()
+    r.tables[me_x] = jnp.zeros((8, rows), f32)
+    r.tables[me_x, 0:2, :] = r.choice_ref[...].astype(f32)
+    r.tables[me_x, 2:4, :] = r.share_ref[...]
+
+    for load in loads[:-2]:
+        load.wait()
+    pl.semaphore_wait(barrier, len(peers))
+
+    def matrix_block(way, event, k, sub):
+        piece = ((event % 2) ^ way) * 2 + sub
+        block = (columns - k if way == 0 else k) % columns
+        return r.matrix.at[block, pl.ds(pl.multiple_of(mine + piece * (rows // 4), 16), rows // 4), on_ring]
+
+    def matrix_ring(way, event, sub):
+        k = event // 2
+        return remote(
+            matrix_block(way, event, k, sub),
+            matrix_block(way, event, k + 1, sub),
+            r.ring_send.at[0],
+            r.ring_recv.at[way, event, sub],
+            toward(way),
+        )
+
+    def slab_copy(offset):
+        return remote(
+            r.matrix.at[0, slab_rows(me_y), on_grid],
+            r.matrix.at[columns - offset, slab_rows(me_y), on_grid],
+            r.slab_send.at[0],
+            r.slab_recv.at[0],
+            {"tp": column(offset)},
+        )
+
+    def grid_view(way, event, y):
+        blocks_of = pl.ds(1, half) if (event % 2) ^ way == 0 else pl.ds(1 + half, half - 1)
+        return r.matrix.at[blocks_of, slab_rows(y), on_grid]
+
+    def grid_ring(way, event, y):
+        here = grid_view(way, event, y)
+        return remote(
+            here, here, r.grid_send.at[0], r.grid_recv.at[way, event], peer(1) if way == 0 else peer(chips - 1)
+        )
+
+    def to_mate(here, which):
+        return remote(here, here, r.pass_send.at[which], r.pass_recv.at[which], mate)
+
+    most_columns, other_blocks = pl.ds(0, columns - 1), pl.ds(1, columns - 1)
+    ring_total = r.matrix.at[other_blocks, pl.ds(0, rows), on_ring]
+    grid_total = r.matrix.at[other_blocks, pl.ds(0, (chips - 1) * slab), on_grid]
+    slab_total = r.matrix.at[other_blocks, pl.ds(0, slab), on_grid]
+    pass_totals = (ring_total, r.matrix.at[other_blocks, pl.ds(0, rows), on_grid])
+
+    rim_rows = 16
+    positions = blocks * rows
+    rims = [
+        remote(
+            r.value_in.at[pl.ds(2 * positions - rim_rows, rim_rows), :],
+            r.value_rim,
+            r.rim_send.at[0],
+            r.rim_recv.at[0],
+            following,
+        ),
+        remote(
+            r.keys_in.at[pl.ds(positions - rim_rows, rim_rows), :], r.keys_rim, r.rim_send.at[1], r.rim_recv.at[1], following
+        ),
+    ]
+    for rim in rims:
+        rim.start()
+
+    def table_copy(offset):
+        here = r.tables.at[me_x]
+        return remote(here, here, r.table_send.at[0], r.table_recv.at[0], {"tp": column(offset)})
+
+    for i in range(1, columns):
+        table_copy(i).start()
+    for i in range(1, columns):
+        slab_copy(i).start()
+    for event in range(min(2, columns - 1)):
+        for sub in range(2):
+            for way in range(2):
+                matrix_ring(way, event, sub).start()
+    tables_total = remote(
+        r.tables.at[most_columns], r.tables.at[most_columns], r.table_send.at[0], r.table_recv.at[0], right
+    )
+
+    def serve_ring(event):
+        for sub in range(2):
+            for way in range(2):
+                matrix_ring(way, event, sub).wait_recv()
+                if event + 2 < columns - 1:
+                    matrix_ring(way, event + 2, sub).start()
+                to_mate(matrix_block(way, event, event // 2 + 1, sub), 0).start()
+
+    def serve_slab():
+        remote(slab_total, slab_total, r.slab_send.at[0], r.slab_recv.at[0], right).wait_recv()
+        for event in range(2):
+            for way in range(2):
+                if event < chips - 1:
+                    grid_ring(way, event, me_y).start()
+        to_mate(r.matrix.at[other_blocks, slab_rows(me_y), on_grid], 1).start()
+
+    def serve_grid(event):
+        k = event // 2 + 1
+        for way in range(2):
+            y = lax.rem(me_y + (chips - k if way == 0 else k), chips)
+            grid_ring(way, event, y).wait_recv()
+            if event + 2 < chips - 1:
+                grid_ring(way, event + 2, y).start()
+            to_mate(grid_view(way, event, y), 1).start()
+
+    waiting = [("x", e) for e in range(columns - 1)] + [("y", e) for e in range(chips - 1)]
+
+    def serve(*steps):
+        for step in steps:
+            if step in waiting:
+                waiting.remove(step)
+                (serve_ring if step[0] == "x" else serve_grid)(step[1])
+
     for t in range(dims.tiles):
         span = pl.ds(t * 128, 128)
         for n, weight in enumerate((r.expert_gate_hbm, r.expert_up_hbm)):
@@ -82,11 +205,6 @@
         pltpu.make_async_copy(
             r.expert_down_hbm.at[0, :, pl.ds(p * PIECE, PIECE)], r.down.at[p], r.weight_sem.at[1]
         ).start()
-
-    barrier = pltpu.get_barrier_semaphore()
-    peers = [{"tp": column(i)} for i in range(1, columns)] + [{"sp": place(i)} for i in range(1, places)]
-    for device in peers:
-        pl.semaphore_signal(barrier, inc=1, device_id=device, device_id_type=MESH)
 
     for g in range(2):
         raw = r.raw_ref[g].astype(f32)
@@ -128,122 +246,6 @@
         low = table[pl.ds(HEADS * k + 2 * g, 1), :]
         high = table[pl.ds(HEADS * k + 2 * g + 1, 1), :]
         return jnp.where(first_head[0:1], low, high)
-
-    r.tables[me_x] = jnp.zeros((8, rows), f32)
-    r.tables[me_x, 0:2, :] = r.choice_ref[...].astype(f32)
-    r.tables[me_x, 2:4, :] = r.share_ref[...]
-
-    for load in loads[:-1]:
-        load.wait()
-    pl.semaphore_wait(barrier, len(peers))
-
-    def matrix_block(way, event, k):
-        piece = (event % 2) ^ way
-        block = (columns - k if way == 0 else k) % columns
-        return r.matrix.at[block, pl.ds(pl.multiple_of(mine + piece * (rows // 2), 16), rows // 2), on_ring]
-
-    def matrix_ring(way, event):
-        k = event // 2
-        return remote(
-            matrix_block(way, event, k),
-            matrix_block(way, event, k + 1),
-            r.ring_send.at[0],
-            r.ring_recv.at[way, event],
-            toward(way),
-        )
-
-    def slab_copy(offset):
-        return remote(
-            r.matrix.at[0, slab_rows(me_y), on_grid],
-            r.matrix.at[columns - offset, slab_rows(me_y), on_grid],
-            r.slab_send.at[0],
-            r.slab_recv.at[0],
-            {"tp": column(offset)},
-        )
-
-    def grid_view(way, event, y):
-        blocks_of = pl.ds(1, half) if (event % 2) ^ way == 0 else pl.ds(1 + half, half - 1)
-        return r.matrix.at[blocks_of, slab_rows(y), on_grid]
-
-    def grid_ring(way, event, y):
-        here = grid_view(way, event, y)
-        return remote(
-            here, here, r.grid_send.at[0], r.grid_recv.at[way, event], peer(1) if way == 0 else peer(chips - 1)
-        )
-
-    def to_mate(here, which):
-        return remote(here, here, r.pass_send.at[which], r.pass_recv.at[which], mate)
-
-    most_columns, other_blocks = pl.ds(0, columns - 1), pl.ds(1, columns - 1)
-    ring_total = r.matrix.at[other_blocks, pl.ds(0, rows), on_ring]
-    grid_total = r.matrix.at[other_blocks, pl.ds(0, (chips - 1) * slab), on_grid]
-    slab_total = r.matrix.at[other_blocks, pl.ds(0, slab), on_grid]
-    pass_totals = (ring_total, r.matrix.at[other_blocks, pl.ds(0, rows), on_grid])
-
-    rim_rows = 16
-    positions = blocks * rows
-    rims = [
-        remote(
-            r.value_in.at[pl.ds(2 * positions - rim_rows, rim_rows), :],
-            r.value_rim,
-            r.rim_send.at[0],
-            r.rim_recv.at[0],
-            following,
-        ),
-        remote(
-            r.keys_in.at[pl.ds(positions - rim_rows, rim_rows), :], r.keys_rim, r.rim_send.at[1], r.rim_recv.at[1], following
-        ),
-    ]
-    for rim in rims:
-        rim.start()
-
-    def table_copy(offset):
-        here = r.tables.at[me_x]
-        return remote(here, here, r.table_send.at[0], r.table_recv.at[0], {"tp": column(offset)})
-
-    for i in range(1, columns):
-        table_copy(i).start()
-    for i in range(1, columns):
-        slab_copy(i).start()
-    for event in range(2):
-        for way in range(2):
-            if event < columns - 1:
-                matrix_ring(way, event).start()
-    tables_total = remote(
-        r.tables.at[most_columns], r.tables.at[most_columns], r.table_send.at[0], r.table_recv.at[0], right
-    )
-
-    def serve_ring(event):
-        for way in range(2):
-            matrix_ring(way, event).wait_recv()
-            if event + 2 < columns - 1:
-                matrix_ring(way, event + 2).start()
-            to_mate(matrix_block(way, event, event // 2 + 1), 0).start()
-
-    def serve_slab():
-        remote(slab_total, slab_total, r.slab_send.at[0], r.slab_recv.at[0], right).wait_recv()
-        for event in range(2):
-            for way in range(2):
-                if event < chips - 1:
-                    grid_ring(way, event, me_y).start()
-        to_mate(r.matrix.at[other_blocks, slab_rows(me_y), on_grid], 1).start()
-
-    def serve_grid(event):
-        k = event // 2 + 1
-        for way in range(2):
-            y = lax.rem(me_y + (chips - k if way == 0 else k), chips)
-            grid_ring(way, event, y).wait_recv()
-            if event + 2 < chips - 1:
-                grid_ring(way, event + 2, y).start()
-            to_mate(grid_view(way, event, y), 1).start()
-
-    waiting = [("x", e) for e in range(columns - 1)] + [("y", e) for e in range(chips - 1)]
-
-    def serve(*steps):
-        for step in steps:
-            if step in waiting:
-                waiting.remove(step)
-                (serve_ring if step[0] == "x" else serve_grid)(step[1])
 
     r.value_wide[rim_rows:, :] = r.value_in[...].astype(f32)
     r.keys_wide[rim_rows:, :] = r.keys_in[...].astype(f32)
@@ -394,7 +396,8 @@
 
     lax.fori_loop(0, columns, put_step, 0)
 
-    loads[-1].wait()
+    for load in loads[-2:]:
+        load.wait()
     serve(*dims.serving[1])
     for n in range(1, chips):
 
@@ -499,7 +502,7 @@
     for block in range(columns):
         product(block, block == 0)
 
-    stream = (r.residual_ref[...].astype(f32) + r.acc_s[...]).astype(bf16)
+    stream = (r.residual_in[...].astype(f32) + r.acc_s[...]).astype(bf16)
     r.stream_s[...] = stream
     wide = stream.astype(f32)
     scale = lax.rsqrt(jnp.mean(wide * wide, axis=1, keepdims=True) + EPSILON)
@@ -519,8 +522,10 @@
     for q in range(extra):
         r.tokens[me_x, q] = normed[:, (direct + q) * PIECE : (direct + q + 1) * PIECE]
 
+    thin = extra * lanes_of
+
     def token_ring(way, step, q, col):
-        here = r.tokens.at[col, q]
+        here = r.tokens.at[col, q // lanes_of, :, pl.ds(q % lanes_of * 128, 128)]
         return remote(here, here, r.token_send.at[0], r.token_recv.at[way, step, q], toward(way))
 
     put_own = r.put[me_x]
@@ -529,7 +534,7 @@
         r.outbound[p] = part[:slots].astype(bf16)
         for c in range(lanes_of):
             r.over_out[:, p * lanes_of + c, :] = part[slots:, c * 128 : (c + 1) * 128]
-    for q in range(extra):
+    for q in range(thin):
         for way in range(2):
             token_ring(way, 0, q, me_x).start()
 
@@ -615,7 +620,7 @@
     route(0)
 
     def token_event(k):
-        for q in range(extra):
+        for q in range(thin):
             for way in range(2):
                 if k <= far(way, q):
                     col = column(-k if way == 0 else k)
@@ -666,7 +671,7 @@
 
     heads_total.wait_send()
     tables_total.wait_send()
-    remote(ring_total, ring_total, r.ring_send.at[0], r.ring_recv.at[0, 0], right).wait_send()
+    remote(ring_total, ring_total, r.ring_send.at[0], r.ring_recv.at[0, 0, 0], right).wait_send()
     remote(slab_total, slab_total, r.slab_send.at[0], r.slab_recv.at[0], right).wait_send()
     remote(grid_total, grid_total, r.grid_send.at[0], r.grid_recv.at[0, 0], right).wait_send()
     for which in range(2):
@@ -839,11 +844,12 @@
             ).start()
         return carry
 
-    def weighted(col, table, q):
-        one = jnp.dot(r.pick[col, 0], table[q], preferred_element_type=f32)
-        two = jnp.dot(r.pick[col, 1], table[q], preferred_element_type=f32)
-        first, second = r.share_s[col, 0], r.share_s[col, 1]
-        return jnp.concatenate([first] * lanes_of, axis=1) * one + jnp.concatenate([second] * lanes_of, axis=1) * two
+    def weighted(col, table):
+        one = jnp.dot(r.pick[col, 0], table, preferred_element_type=f32)
+        two = jnp.dot(r.pick[col, 1], table, preferred_element_type=f32)
+        copies = one.shape[1] // 128
+        first, second = (jnp.concatenate([r.share_s[col, k]] * copies, axis=1) for k in range(2))
+        return first * one + second * two
 
     def take_back(offset):
         col = column(offset)
@@ -856,10 +862,9 @@
                 ].astype(bf16)
 
     def token_hop(way, j, q):
-        buffer = r.xsum_right if way == 0 else r.xsum_left
         return remote(
-            buffer.at[j, q],
-            buffer.at[j - 1, q],
+            r.xsums.at[way, j, q],
+            r.xsums.at[way, j - 1, q],
             r.xsum_send.at[0],
             r.xsum_recv.at[way, j - 1, q],
             toward(way),
@@ -867,10 +872,12 @@
 
     taken = set()
 
+    def thin_part(col, q):
+        return weighted(col, r.xret[col, q // lanes_of, :, q % lanes_of * 128 : (q % lanes_of + 1) * 128])
+
     def token_round(t):
-        for q in range(extra):
+        for q in range(thin):
             for way in range(2):
-                buffer = r.xsum_right if way == 0 else r.xsum_left
                 j = far(1 - way, q) - t
                 if j < 1:
                     continue
@@ -878,12 +885,11 @@
                 if offset not in taken:
                     taken.add(offset)
                     take_back(offset)
-                col = column(offset)
-                value = weighted(col, r.xret.at[col], q)
+                value = thin_part(column(offset), q)
                 if t > 0:
                     token_hop(way, j + 1, q).wait_recv()
-                    value = value + buffer[j, q].astype(f32)
-                buffer[j, q] = value.astype(bf16)
+                    value = value + r.xsums[way, j, q].astype(f32)
+                r.xsums[way, j, q] = value.astype(bf16)
                 token_hop(way, j, q).start()
 
     for group in dims.groups:
@@ -923,14 +929,18 @@
     left_by_now(r.chunks.at[most_columns, pl.ds(0, direct)], r.sum_send.at[0], r.sum_recv.at[0, 0, 0])
     token_round(half - 1)
     take_back(0)
-    for q in range(extra):
-        value = weighted(me_x, r.xret.at[me_x], q)
+    for q in range(thin):
+        value = thin_part(me_x, q)
         for way in range(2):
             token_hop(way, 1, q).wait_recv()
-        value = value + r.xsum_right[0, q].astype(f32) + r.xsum_left[0, q].astype(f32)
-        span = slice((direct + q) * PIECE, (direct + q + 1) * PIECE)
-        r.out_ref[:, span] = (r.stream_s[:, span].astype(f32) + value).astype(bf16)
-
+            value = value + r.xsums[way, 0, q].astype(f32)
+        span = slice(direct * PIECE + q * 128, direct * PIECE + (q + 1) * 128)
+        r.out_s[:, span] = (r.stream_s[:, span].astype(f32) + value).astype(bf16)
+
+    def write_out(span):
+        return pltpu.make_async_copy(r.out_s.at[:, span], r.out_ref.at[:, span], r.done_sem.at[0])
+
+    write_out(pl.ds(direct * PIECE, extra * PIECE)).start()
     remote(
         r.over_back.at[0 : places - 1], r.over_ret.at[0 : places - 1], r.over_send.at[1], r.over_recv.at[1], right
     ).wait_recv()
@@ -947,8 +957,9 @@
     def combine(p, carry):
         back_arrived(p).wait_recv()
         span = pl.ds(pl.multiple_of(p * PIECE, PIECE), PIECE)
-        value = weighted(me_x, r.returned, p)
-        r.out_ref[:, span] = (r.stream_s[:, span].astype(f32) + value).astype(bf16)
+        value = weighted(me_x, r.returned[p])
+        r.out_s[:, span] = (r.stream_s[:, span].astype(f32) + value).astype(bf16)
+        write_out(span).start()
         return carry
 
     lax.fori_loop(0, direct, combine, 0)
@@ -956,11 +967,12 @@
     left_by_now(r.over_back.at[most_places], r.over_send.at[1], r.over_recv.at[1])
     left_by_now(r.tokens.at[most_columns], r.xsum_send.at[0], r.xsum_recv.at[0, 0, 0])
     left_by_now(r.totals.at[:, most_lines, :], r.back_send.at[0], r.back_recv.at[0])
+    pltpu.make_async_copy(r.out_s, r.out_ref, r.done_sem.at[0]).wait()
 
 
 def layer(places, columns, **given):
     f32, bf16 = jnp.float32, jnp.bfloat16
-    rows, width = given["residual_ref"].shape
+    rows, width = given["residual_hbm"].shape
     units = given["expert_gate_hbm"].shape[2]
     lanes = given["keys_hbm"].shape[1]
     positions = columns * BLOCK
@@ -976,23 +988,37 @@
     opening = (1, 0, 2, -1, -2, 3, -3, -4, 4, -5) if half == 4 else (*range(1, half + 1), *range(0, -direct, -1))
     serving = [
         [("x", 0)],
-        [("x", 1), ("y", 0)],
-        [("x", 2), ("y", 1)],
-        [("x", 3), ("y", 2), ("x", 4), ("y", 3), ("y", 4), ("y", 5), ("x", 5), ("x", 6), ("y", 6)],
+        [("x", 1)],
+        [("x", 2)],
+        [("x", 3), ("y", 0), ("y", 1), ("y", 2), ("x", 4), ("y", 3), ("y", 4), ("y", 5), ("x", 5), ("x", 6), ("y", 6)],
     ]
-    groups = [(low, min(low + 2, direct)) for low in range(0, direct, 2)]
-    closing = []
-    for n, group in enumerate(groups):
-        last = n == len(groups) - 1
+    low, high = (0, (direct + 1) // 2), ((direct + 1) // 2, direct)
+    groups = [high, low]
+    if half == 4:
+        closing = [
+            ("long", 1, high),
+            ("short", 1, high),
+            ("long", 1, low),
+            ("short", 1, low),
+            ("long", 2, low),
+            ("long", 2, high),
+            ("long", 3, low),
+            ("short", 2, low),
+            ("token", 0, None),
+            ("long", 3, high),
+            ("finish", None, low),
+            ("short", 2, high),
+            ("token", 1, None),
+            ("finish", None, high),
+            ("token", 2, None),
+        ]
+    else:
+        closing = []
         for step in range(1, half):
-            if step < half - 1:
-                closing.append(("short", step, group))
-            closing.append(("long", step, group))
-            if last and step < half:
-                closing.append(("token", step - 1, None))
-        if n > 0:
-            closing.insert(len(closing) - half, ("finish", None, groups[n - 1]))
-    closing.append(("finish", None, groups[-1]))
+            closing += [("short", step, group) for group in groups if step < half - 1]
+            closing += [("long", step, group) for group in groups]
+            closing.append(("token", step - 1, None))
+        closing += [("finish", None, group) for group in groups]
     dims = types.SimpleNamespace(
         places=places, columns=columns, width=width, main=main, over=over, pieces=pieces, direct=direct, tiles=tiles,
         schedule=schedule, opening=opening, groups=groups, closing=closing, ring_part=ring_part, serving=serving,
@@ -1007,6 +1033,7 @@
     ]
     lane_rows = PIECE // 128
     scratch = dict(
+        residual_in=vmem(rows, width),
         value_in=vmem(2 * positions, BLOCK),
         gate_in=vmem(2 * positions, BLOCK),
         keys_in=vmem(positions, lanes),
@@ -1041,6 +1068,7 @@
         matrix=vmem(columns, 2 * BLOCK, width),
         acc_s=vmem(rows, width, dtype=f32),
         stream_s=vmem(rows, width),
+        out_s=vmem(rows, width),
         tables=vmem(columns, 8, rows, dtype=f32),
         put=vmem(columns, total, rows),
         pick=vmem(columns, 2, rows, total),
@@ -1064,12 +1092,12 @@
         gate_up=vmem(tiles, width, 256),
         down=vmem(pieces, units, PIECE),
         sums=vmem(2, half + 1, direct, total, PIECE),
-        xsum_right=vmem(half + 1, extra, rows, PIECE),
-        xsum_left=vmem(half + 1, extra, rows, PIECE),
+        xsums=vmem(2, half + 1, extra * lane_rows, rows, 128),
         totals=vmem(direct, places * main, PIECE),
         returned=vmem(direct, total, PIECE),
-        load_sem=dma(5),
+        load_sem=dma(6),
         weight_sem=dma(2),
+        done_sem=dma(1),
     )
     steps = (2, half)
     for name, send, recv in (
@@ -1079,12 +1107,12 @@
         ("enter", (1,), (1,)),
         ("head", (1,), (1,)),
         ("table", (1,), (1,)),
-        ("ring", (1,), (2, columns - 1)),
+        ("ring", (1,), (2, columns - 1, 2)),
         ("slab", (1,), (1,)),
         ("grid", (1,), (2, chips - 1)),
         ("pass", (2,), (2,)),
         ("over", (2,), (2,)),
-        ("token", (1,), (*steps, extra)),
+        ("token", (1,), (*steps, extra * lane_rows)),
         ("out", (1,), (direct,)),
         ("xout", (1,), (columns,)),
         ("xover", (2,), (2, columns)),
@@ -1092,7 +1120,7 @@
         ("tail", (1,), steps),
         ("xback", (1,), (columns,)),
         ("sum", (1,), (*steps, direct)),
-        ("xsum", (1,), (*steps, extra)),
+        ("xsum", (1,), (*steps, extra * lane_rows)),
         ("back", (1,), (direct,)),
     ):
         scratch[name + "_send"], scratch[name + "_recv"] = dma(*send), dma(*recv)
@@ -1101,7 +1129,7 @@
         functools.partial(layer_kernel, dims, names),
         out_shape=jax.ShapeDtypeStruct((rows, width), bf16),
         in_specs=in_specs,
-        out_specs=pl.BlockSpec(memory_space=pltpu.VMEM),
+        out_specs=pl.BlockSpec(memory_space=pl.ANY),
         scratch_shapes=list(scratch.values()),
         compiler_params=pltpu.CompilerParams(
             collective_id=0, has_side_effects=True, vmem_limit_bytes=VMEM_LIMIT
@@ -1134,7 +1162,7 @@
     return layer(
         lax.axis_size("sp"),
         lax.axis_size("tp"),
-        residual_ref=residual,
+        residual_hbm=residual,
         value_hbm=grouped_value_heads.reshape(-1, BLOCK),
         gate_hbm=output_gate_heads.reshape(-1, BLOCK),
         keys_hbm=projected_key_query,

time: 230 us -> 223 us (0.970)
  Pallas kernels: 228 us -> 221 us
    pallas_call x1, Pallas kernels: 228 us -> 221 us  [layer(): pl.pallas_call(functools.partial(layer_kernel, dims, names), out_shape=ja...]
where the time goes in v3:
time: 223 us; the launch traced here: 222 us
  Pallas kernels  221 us (99%)
    pallas_call x1, Pallas kernels, layer(): pl.pallas_call(functools.partial(layer_kernel, dims, names), out_shape=ja...  221 us

profile of v3, /device:TPU:513, one launch (start us, length us, event | category | flops | bytes accessed | tf_op | source)
XLA Modules:
  0.0 222.4 jit_solution(11281373633893334251)
XLA Ops:
  0.0 220.5 %layer.1 = bf16[128,2048]{1,0:T(8,128)(2,1)} custom-call(bf16[128,2048]{1,0:T(8,128)(2,1)} %refs_0_.1, bf16[2048,128]{1,0:T(8,128)(2,1)} %bitcast.8, bf16[2048,128]{1,0:T(8,128)(2,1)} %bitcast.9, bf16[1024,384]{1,0:T(8,128)(2,1)} %refs_3_.1, bf16[2,2,1024]{2,1,0:T(2,128)(2,1)} %bitcast.10, f32[2,2]{1,0:T(2,128)} %refs_5_.1, f32[2,2]{1,0:T(2,128)} %refs_6_.1, ...), custom_call_target="tpu_custom_call" | custom-call | tf_op jit(solution)/shard_map/layer/pallas_call | solution.py:1128
  220.6 1.9 copy.21

commit v4 on v3

--- a/solution.py
+++ b/solution.py
@@ -60,6 +60,10 @@
     for device in peers:
         pl.semaphore_signal(barrier, inc=1, device_id=device, device_id_type=MESH)
 
+    small = {
+        name: pltpu.make_async_copy(getattr(r, name), getattr(r, name[:-5] + "ref"), r.small_sem.at[n])
+        for n, name in enumerate(dims.small)
+    }
     ring_part, slab = dims.ring_part, rows // chips
     mine = pl.multiple_of(core * rows, rows)
 
@@ -76,13 +80,15 @@
         (r.residual_hbm, r.residual_in),
     ]
     loads = [pltpu.make_async_copy(a, b, r.load_sem.at[n]) for n, (a, b) in enumerate(loads)]
-    for load in loads:
+    for load in loads[:2] + list(small.values()) + loads[2:]:
         load.start()
+    for name in ("choice_small", "share_small"):
+        small[name].wait()
     r.tables[me_x] = jnp.zeros((8, rows), f32)
     r.tables[me_x, 0:2, :] = r.choice_ref[...].astype(f32)
     r.tables[me_x, 2:4, :] = r.share_ref[...]
 
-    for load in loads[:-2]:
+    for load in loads[:2]:
         load.wait()
     pl.semaphore_wait(barrier, len(peers))
 
@@ -97,7 +103,7 @@
             matrix_block(way, event, k, sub),
             matrix_block(way, event, k + 1, sub),
             r.ring_send.at[0],
-            r.ring_recv.at[way, event, sub],
+            r.ring_recv.at[event, sub],
             toward(way),
         )
 
@@ -117,7 +123,7 @@
     def grid_ring(way, event, y):
         here = grid_view(way, event, y)
         return remote(
-            here, here, r.grid_send.at[0], r.grid_recv.at[way, event], peer(1) if way == 0 else peer(chips - 1)
+            here, here, r.grid_send.at[0], r.grid_recv.at[event], peer(1) if way == 0 else peer(chips - 1)
         )
 
     def to_mate(here, which):
@@ -129,6 +135,8 @@
     slab_total = r.matrix.at[other_blocks, pl.ds(0, slab), on_grid]
     pass_totals = (ring_total, r.matrix.at[other_blocks, pl.ds(0, rows), on_grid])
 
+    for load in loads[2:4]:
+        load.wait()
     rim_rows = 16
     positions = blocks * rows
     rims = [
@@ -164,8 +172,9 @@
 
     def serve_ring(event):
         for sub in range(2):
+            both = r.matrix.at[0, pl.ds(0, rows // 2), on_ring]
+            remote(both, both, r.ring_send.at[0], r.ring_recv.at[event, sub], right).wait_recv()
             for way in range(2):
-                matrix_ring(way, event, sub).wait_recv()
                 if event + 2 < columns - 1:
                     matrix_ring(way, event + 2, sub).start()
                 to_mate(matrix_block(way, event, event // 2 + 1, sub), 0).start()
@@ -180,9 +189,9 @@
 
     def serve_grid(event):
         k = event // 2 + 1
+        remote(slab_total, slab_total, r.grid_send.at[0], r.grid_recv.at[event], right).wait_recv()
         for way in range(2):
             y = lax.rem(me_y + (chips - k if way == 0 else k), chips)
-            grid_ring(way, event, y).wait_recv()
             if event + 2 < chips - 1:
                 grid_ring(way, event + 2, y).start()
             to_mate(grid_view(way, event, y), 1).start()
@@ -206,6 +215,9 @@
             r.expert_down_hbm.at[0, :, pl.ds(p * PIECE, PIECE)], r.down.at[p], r.weight_sem.at[1]
         ).start()
 
+    for name in dims.small:
+        if name not in ("choice_small", "share_small"):
+            small[name].wait()
     for g in range(2):
         raw = r.raw_ref[g].astype(f32)
         for k in range(blocks):
@@ -336,7 +348,11 @@
     def to_chip(n, which):
         src = r.chip_pack.at[my_half, :] if which == 0 else r.chip_fade
         dst = r.all_pack.at[me_y] if which == 0 else r.all_fade.at[me_y]
-        return remote(src, dst, r.chip_send.at[which, n], r.chip_recv.at[which, n], peer(n))
+        return remote(src, dst, r.chip_send.at[n], r.chip_recv.at[n], peer(n))
+
+    def chip_total(n):
+        sent = r.own_pack.at[pl.ds(0, piece + 16), :]
+        return remote(sent, sent, r.chip_send.at[n], r.chip_recv.at[n], peer(n))
 
     for n in range(1, chips):
 
@@ -403,8 +419,7 @@
 
         @pl.when(me_y >= n)
         def _():
-            for which in range(2):
-                to_chip(n, which).wait_recv()
+            chip_total(n).wait_recv()
 
     row_at = lax.broadcasted_iota(jnp.int32, (piece, rows), 0) + core * piece
     half_two = row_at < STATE_TWO
@@ -485,22 +500,25 @@
             r.pick[col, k] = jnp.where(rank_x == turn_t, named_x, 0.0).astype(bf16)
             r.share_s[col, k] = jnp.broadcast_to(table[:, 2 + k : 3 + k], (rows, rows))
 
-    def product(block, first):
-        for n in range(0, width, 512):
-            span = slice(n, n + 512)
+    def product(block, low, high, first):
+        for n in range(low, high, 512):
+            span = slice(n, min(n + 512, high))
             part = jnp.dot(r.heads_in[column(block)], r.matrix[block, :, span], preferred_element_type=f32)
             r.acc_s[:, span] = part if first else r.acc_s[:, span] + part
 
     serve(*dims.serving[3])
-    serve(*list(waiting))
+    serve(*[step for step in waiting if step[0] == "y"])
     heads_total = remote(
         r.mixed_s.at[most_columns], r.heads_in.at[most_columns], r.head_send.at[0], r.head_recv.at[0], right
     )
     heads_total.wait_recv()
-    remote(pass_totals[0], pass_totals[0], r.pass_send.at[0], r.pass_recv.at[0], mate).wait_recv()
     remote(pass_totals[1], pass_totals[1], r.pass_send.at[1], r.pass_recv.at[1], mate).wait_recv()
     for block in range(columns):
-        product(block, block == 0)
+        product(block, ring_part, width, block == 0)
+    serve(*list(waiting))
+    remote(pass_totals[0], pass_totals[0], r.pass_send.at[0], r.pass_recv.at[0], mate).wait_recv()
+    for block in range(columns):
+        product(block, 0, ring_part, block == 0)
 
     stream = (r.residual_in[...].astype(f32) + r.acc_s[...]).astype(bf16)
     r.stream_s[...] = stream
@@ -526,17 +544,15 @@
 
     def token_ring(way, step, q, col):
         here = r.tokens.at[col, q // lanes_of, :, pl.ds(q % lanes_of * 128, 128)]
-        return remote(here, here, r.token_send.at[0], r.token_recv.at[way, step, q], toward(way))
+        return remote(here, here, r.token_send.at[0], r.token_recv.at[step, q], toward(way))
 
     put_own = r.put[me_x]
-    for p in range(direct):
+
+    def make_out(p):
         part = jnp.dot(put_own, normed[:, p * PIECE : (p + 1) * PIECE], preferred_element_type=f32)
         r.outbound[p] = part[:slots].astype(bf16)
         for c in range(lanes_of):
             r.over_out[:, p * lanes_of + c, :] = part[slots:, c * 128 : (c + 1) * 128]
-    for q in range(thin):
-        for way in range(2):
-            token_ring(way, 0, q, me_x).start()
 
     def send_out(p, carry):
         for i in range(1, places):
@@ -550,7 +566,14 @@
         r.chunks[me_x, p, lines(me_s), :] = r.outbound[p, lines(me_s), :]
         return carry
 
-    lax.fori_loop(0, direct, send_out, 0)
+    make_out(0)
+    send_out(0, 0)
+    for q in range(thin):
+        for way in range(2):
+            token_ring(way, 0, q, me_x).start()
+    for p in range(1, direct):
+        make_out(p)
+    lax.fori_loop(1, direct, send_out, 0)
     for i in range(1, places):
         remote(
             r.over_out.at[place(i)], r.over_in.at[me_s], r.over_send.at[0], r.over_recv.at[0], {"sp": place(i)}
@@ -558,7 +581,7 @@
     r.over_in[me_s] = r.over_out[me_s]
     if places < over:
         r.over_in[places:over] = jnp.zeros((over - places, *r.over_in.shape[1:]), f32)
-        r.over_ret[places:over] = jnp.zeros((over - places, *r.over_ret.shape[1:]), f32)
+        r.over_ret[:, places:over] = jnp.zeros((2, over - places, *r.over_ret.shape[2:]), f32)
         r.xover_in[:, places:over] = jnp.zeros((columns, over - places, *r.xover_in.shape[2:]), f32)
         r.xover_ret[:, places:over] = jnp.zeros((columns, over - places, *r.xover_ret.shape[2:]), f32)
 
@@ -621,23 +644,22 @@
 
     def token_event(k):
         for q in range(thin):
+            came = r.tokens.at[pl.ds(0, 2 if k < half else 1), 0, :, pl.ds(0, 128)]
+            remote(came, came, r.token_send.at[0], r.token_recv.at[k - 1, q], right).wait_recv()
             for way in range(2):
-                if k <= far(way, q):
-                    col = column(-k if way == 0 else k)
-                    token_ring(way, k - 1, q, col).wait_recv()
-                    if k < far(way, q):
-                        token_ring(way, k, q, col).start()
+                if k < far(way, q):
+                    token_ring(way, k, q, column(-k if way == 0 else k)).start()
         if k < half:
             route(columns - k)
         route(k)
 
     def chunk_ring(way, step, p, col):
         here = r.chunks.at[col, p, pl.ds(0, slots), :]
-        return remote(here, here, r.chunk_send.at[0], r.chunk_recv.at[way, step, p], toward(way))
+        return remote(here, here, r.chunk_send.at[0], r.chunk_recv.at[step, p], toward(way))
 
     def over_ring(way, step, col):
         here = r.chunks.at[col, pl.ds(0, direct), pl.ds(slots, over), :]
-        return remote(here, here, r.tail_send.at[0], r.tail_recv.at[way, step], toward(way))
+        return remote(here, here, r.tail_send.at[0], r.tail_recv.at[step], toward(way))
 
     def out_arrived(p):
         most = pl.ds(0, (places - 1) * main)
@@ -666,14 +688,13 @@
 
         @pl.when(me_y + n < chips)
         def _():
-            for which in range(2):
-                to_chip(n, which).wait_send()
+            chip_total(n).wait_send()
 
     heads_total.wait_send()
     tables_total.wait_send()
-    remote(ring_total, ring_total, r.ring_send.at[0], r.ring_recv.at[0, 0, 0], right).wait_send()
+    remote(ring_total, ring_total, r.ring_send.at[0], r.ring_recv.at[0, 0], right).wait_send()
     remote(slab_total, slab_total, r.slab_send.at[0], r.slab_recv.at[0], right).wait_send()
-    remote(grid_total, grid_total, r.grid_send.at[0], r.grid_recv.at[0, 0], right).wait_send()
+    remote(grid_total, grid_total, r.grid_send.at[0], r.grid_recv.at[0], right).wait_send()
     for which in range(2):
         view = pass_totals[which]
         remote(view, view, r.pass_send.at[which], r.pass_recv.at[which], mate).wait_send()
@@ -796,18 +817,15 @@
                 chains(False, 0, group)
 
         def pass_on(p, carry, k=k, first=first, last=last):
-            for way in range(2):
-                col = column(-k if way == 0 else k)
-
-                @pl.when(k <= far(way, p))
-                def _():
-                    chunk_ring(way, k - 1, p, col).wait_recv()
-
-                if k < half:
-
-                    @pl.when(k < far(way, p))
-                    def _():
-                        chunk_ring(way, k, p, col).start()
+            came = r.chunks.at[pl.ds(0, 2 if k < half else 1), p, pl.ds(0, slots), :]
+            remote(came, came, r.chunk_send.at[0], r.chunk_recv.at[k - 1, p], right).wait_recv()
+            if k < half:
+                for way in range(2):
+                    start = lambda way=way: chunk_ring(way, k, p, column(-k if way == 0 else k)).start()
+                    if k < half - 1:
+                        start()
+                    else:
+                        pl.when(k < far(way, p))(start)
 
             if last > first:
                 units(
@@ -816,12 +834,11 @@
             return carry
 
         lax.fori_loop(0, direct, pass_on, 0)
+        came = r.chunks.at[pl.ds(0, 2 if k < half else 1), pl.ds(0, direct), pl.ds(slots, over), :]
+        remote(came, came, r.tail_send.at[0], r.tail_recv.at[k - 1], right).wait_recv()
         for way in range(2):
-            if k <= far(way, 0):
-                col = column(-k if way == 0 else k)
-                over_ring(way, k - 1, col).wait_recv()
-                if k < far(way, 0):
-                    over_ring(way, k, col).start()
+            if k < far(way, 0):
+                over_ring(way, k, column(-k if way == 0 else k)).start()
         if k == 1:
             lax.fori_loop(0, columns, lambda col, carry: (make_pick(col), carry)[1], 0)
     units(share_of[half] * dims.tiles, columns * dims.tiles)
@@ -900,12 +917,29 @@
     most_places, most_lines = pl.ds(0, places - 1), pl.ds(0, (places - 1) * main)
     chunks_total = r.chunks.at[most_columns, pl.ds(0, direct), pl.ds(0, slots), :]
     left_by_now(r.over_out.at[most_places], r.over_send.at[0], r.over_recv.at[0])
-    left_by_now(r.tokens.at[most_columns], r.token_send.at[0], r.token_recv.at[0, 0, 0])
-    left_by_now(r.chunks.at[most_columns, pl.ds(0, direct), pl.ds(slots, over), :], r.tail_send.at[0], r.tail_recv.at[0, 0])
-    left_by_now(chunks_total, r.chunk_send.at[0], r.chunk_recv.at[0, 0, 0])
+    left_by_now(r.tokens.at[most_columns], r.token_send.at[0], r.token_recv.at[0, 0])
+    left_by_now(r.chunks.at[most_columns, pl.ds(0, direct), pl.ds(slots, over), :], r.tail_send.at[0], r.tail_recv.at[0])
+    left_by_now(chunks_total, r.chunk_send.at[0], r.chunk_recv.at[0, 0])
     left_by_now(r.outbound.at[:, most_lines, :], r.out_send.at[0], r.out_recv.at[0])
     left_by_now(r.xout.at[:, :, most_lines, :], r.xout_send.at[0], r.xout_recv.at[0])
     left_by_now(r.xover_out.at[:, most_places], r.xover_send.at[0], r.xover_recv.at[0, 0])
+    def over_back_copy(n, to, at):
+        return remote(
+            r.over_back.at[n, to],
+            r.over_ret.at[n, at],
+            r.over_send.at[1],
+            r.over_recv.at[1 + n],
+            {"sp": to},
+        )
+
+    def send_over_back(n, group):
+        for p in range(*group):
+            for c in range(lanes_of):
+                r.over_back[n, :, (p - group[0]) * lanes_of + c, :] = r.over_total[p, :, c * 128 : (c + 1) * 128]
+        r.over_ret[n, me_s] = r.over_back[n, me_s]
+        for i in range(1, places):
+            over_back_copy(n, place(i), me_s).start()
+
     for kind, step, group in dims.closing:
         if kind == "short":
             chains(False, step, group)
@@ -915,19 +949,42 @@
             token_round(step)
         else:
             lax.fori_loop(*group, finish, 0)
-    for c in range(direct * lanes_of):
-        at_lanes = (c % lanes_of) * 128
-        r.over_back[:, c, :] = r.over_total[c // lanes_of, :, at_lanes : at_lanes + 128]
-    r.over_ret[me_s] = r.over_back[me_s]
-    for i in range(1, places):
-        remote(
-            r.over_back.at[place(i)], r.over_ret.at[me_s], r.over_send.at[1], r.over_recv.at[1], {"sp": place(i)}
-        ).start()
-
+            send_over_back(dims.groups.index(group), group)
     left_by_now(r.xback.at[:, :, most_lines, :], r.xback_send.at[0], r.xback_recv.at[0])
     left_by_now(r.xover_back.at[:, most_places], r.xover_send.at[1], r.xover_recv.at[1, 0])
     left_by_now(r.chunks.at[most_columns, pl.ds(0, direct)], r.sum_send.at[0], r.sum_recv.at[0, 0, 0])
     token_round(half - 1)
+    def write_out(span):
+        return pltpu.make_async_copy(r.out_s.at[:, span], r.out_ref.at[:, span], r.done_sem.at[0])
+
+    def back_arrived(p):
+        most = pl.ds(0, (places - 1) * main)
+        return remote(
+            r.totals.at[p, most, :], r.returned.at[p, most, :], r.back_send.at[0], r.back_recv.at[p], right
+        )
+
+    def combine(p, carry):
+        back_arrived(p).wait_recv()
+        span = pl.ds(pl.multiple_of(p * PIECE, PIECE), PIECE)
+        value = weighted(me_x, r.returned[p])
+        r.out_s[:, span] = (r.stream_s[:, span].astype(f32) + value).astype(bf16)
+        write_out(span).start()
+        return carry
+
+    def combine_group(n, group):
+        remote(
+            r.over_back.at[n, 0 : places - 1],
+            r.over_ret.at[n, 0 : places - 1],
+            r.over_send.at[1],
+            r.over_recv.at[1 + n],
+            right,
+        ).wait_recv()
+        for p in range(*group):
+            for c in range(lanes_of):
+                r.returned[p, slots:, c * 128 : (c + 1) * 128] = r.over_ret[n, :, (p - group[0]) * lanes_of + c, :].astype(bf16)
+        lax.fori_loop(*group, combine, 0)
+
+    combine_group(dims.groups.index(dims.order[0]), dims.order[0])
     take_back(0)
     for q in range(thin):
         value = thin_part(me_x, q)
@@ -937,34 +994,10 @@
         span = slice(direct * PIECE + q * 128, direct * PIECE + (q + 1) * 128)
         r.out_s[:, span] = (r.stream_s[:, span].astype(f32) + value).astype(bf16)
 
-    def write_out(span):
-        return pltpu.make_async_copy(r.out_s.at[:, span], r.out_ref.at[:, span], r.done_sem.at[0])
-
     write_out(pl.ds(direct * PIECE, extra * PIECE)).start()
-    remote(
-        r.over_back.at[0 : places - 1], r.over_ret.at[0 : places - 1], r.over_send.at[1], r.over_recv.at[1], right
-    ).wait_recv()
-    for c in range(direct * lanes_of):
-        at_lanes = (c % lanes_of) * 128
-        r.returned[c // lanes_of, slots:, at_lanes : at_lanes + 128] = r.over_ret[:, c, :].astype(bf16)
-
-    def back_arrived(p):
-        most = pl.ds(0, (places - 1) * main)
-        return remote(
-            r.totals.at[p, most, :], r.returned.at[p, most, :], r.back_send.at[0], r.back_recv.at[p], right
-        )
-
-    def combine(p, carry):
-        back_arrived(p).wait_recv()
-        span = pl.ds(pl.multiple_of(p * PIECE, PIECE), PIECE)
-        value = weighted(me_x, r.returned[p])
-        r.out_s[:, span] = (r.stream_s[:, span].astype(f32) + value).astype(bf16)
-        write_out(span).start()
-        return carry
-
-    lax.fori_loop(0, direct, combine, 0)
-
-    left_by_now(r.over_back.at[most_places], r.over_send.at[1], r.over_recv.at[1])
+    combine_group(dims.groups.index(dims.order[1]), dims.order[1])
+
+    left_by_now(r.over_back.at[:, most_places], r.over_send.at[1], r.over_recv.at[1])
     left_by_now(r.tokens.at[most_columns], r.xsum_send.at[0], r.xsum_recv.at[0, 0, 0])
     left_by_now(r.totals.at[:, most_lines, :], r.back_send.at[0], r.back_recv.at[0])
     pltpu.make_async_copy(r.out_s, r.out_ref, r.done_sem.at[0]).wait()
@@ -973,6 +1006,7 @@
 def layer(places, columns, **given):
     f32, bf16 = jnp.float32, jnp.bfloat16
     rows, width = given["residual_hbm"].shape
+    small = [name for name in given if name.endswith("_small")]
     units = given["expert_gate_hbm"].shape[2]
     lanes = given["keys_hbm"].shape[1]
     positions = columns * BLOCK
@@ -990,7 +1024,7 @@
         [("x", 0)],
         [("x", 1)],
         [("x", 2)],
-        [("x", 3), ("y", 0), ("y", 1), ("y", 2), ("x", 4), ("y", 3), ("y", 4), ("y", 5), ("x", 5), ("x", 6), ("y", 6)],
+        [("x", 3), ("y", 0), ("y", 1), ("y", 2), ("x", 4), ("y", 3), ("y", 4), ("y", 5), ("y", 6), ("x", 5)],
     ]
     low, high = (0, (direct + 1) // 2), ((direct + 1) // 2, direct)
     groups = [high, low]
@@ -1021,18 +1055,16 @@
         closing += [("finish", None, group) for group in groups]
     dims = types.SimpleNamespace(
         places=places, columns=columns, width=width, main=main, over=over, pieces=pieces, direct=direct, tiles=tiles,
-        schedule=schedule, opening=opening, groups=groups, closing=closing, ring_part=ring_part, serving=serving,
+        schedule=schedule, opening=opening, small=small, groups=groups, order=(low, high), closing=closing, ring_part=ring_part, serving=serving,
     )
     packed = STATE_ONE + STATE_TWO
     square = (blocks, 2, BLOCK, BLOCK)
     vmem = lambda *shape, dtype=bf16: pltpu.VMEM(shape, dtype)
     dma = lambda *shape: pltpu.SemaphoreType.DMA(shape)
-    spaces = {"ref": pltpu.VMEM, "hbm": pl.ANY}
-    in_specs = [
-        pl.BlockSpec(memory_space=pltpu.SMEM if a.shape == (2, 2) else spaces[name[-3:]]) for name, a in given.items()
-    ]
+    in_specs = [pl.BlockSpec(memory_space=pltpu.SMEM if a.shape == (2, 2) else pl.ANY) for a in given.values()]
     lane_rows = PIECE // 128
-    scratch = dict(
+    scratch = {name[:-5] + "ref": pltpu.VMEM(given[name].shape, given[name].dtype) for name in small}
+    scratch |= dict(
         residual_in=vmem(rows, width),
         value_in=vmem(2 * positions, BLOCK),
         gate_in=vmem(2 * positions, BLOCK),
@@ -1077,8 +1109,8 @@
         outbound=vmem(direct, places * main, PIECE),
         over_out=vmem(over, direct * lane_rows, 128, dtype=f32),
         over_in=vmem(over, direct * lane_rows, 128, dtype=f32),
-        over_back=vmem(over, direct * lane_rows, 128, dtype=f32),
-        over_ret=vmem(over, direct * lane_rows, 128, dtype=f32),
+        over_back=vmem(2, over, (high[1] - low[0] + 1) // 2 * lane_rows, 128, dtype=f32),
+        over_ret=vmem(2, over, (high[1] - low[0] + 1) // 2 * lane_rows, 128, dtype=f32),
         over_total=vmem(direct, over, PIECE, dtype=f32),
         xout=vmem(columns, extra, places * main, PIECE),
         xback=vmem(columns, extra, places * main, PIECE),
@@ -1098,26 +1130,27 @@
         load_sem=dma(6),
         weight_sem=dma(2),
         done_sem=dma(1),
+        small_sem=dma(len(small)),
     )
     steps = (2, half)
     for name, send, recv in (
         ("rim", (2,), (2,)),
         ("mate", (2,), (2,)),
-        ("chip", (2, chips), (2, chips)),
+        ("chip", (chips,), (chips,)),
         ("enter", (1,), (1,)),
         ("head", (1,), (1,)),
         ("table", (1,), (1,)),
-        ("ring", (1,), (2, columns - 1, 2)),
+        ("ring", (1,), (columns - 1, 2)),
         ("slab", (1,), (1,)),
-        ("grid", (1,), (2, chips - 1)),
+        ("grid", (1,), (chips - 1,)),
         ("pass", (2,), (2,)),
-        ("over", (2,), (2,)),
-        ("token", (1,), (*steps, extra * lane_rows)),
+        ("over", (2,), (3,)),
+        ("token", (1,), (half, extra * lane_rows)),
         ("out", (1,), (direct,)),
         ("xout", (1,), (columns,)),
         ("xover", (2,), (2, columns)),
-        ("chunk", (1,), (*steps, direct)),
-        ("tail", (1,), steps),
+        ("chunk", (1,), (half, direct)),
+        ("tail", (1,), (half,)),
         ("xback", (1,), (columns,)),
         ("sum", (1,), (*steps, direct)),
         ("xsum", (1,), (*steps, extra * lane_rows)),
@@ -1166,18 +1199,18 @@
         value_hbm=grouped_value_heads.reshape(-1, BLOCK),
         gate_hbm=output_gate_heads.reshape(-1, BLOCK),
         keys_hbm=projected_key_query,
-        raw_ref=raw_step_size.transpose(1, 2, 0),
+        raw_small=raw_step_size.transpose(1, 2, 0),
         bias_ref=step_size_bias,
         log_ref=head_decay_logarithm,
-        extra_ref=position_extra_decay.reshape(-1, BLOCK),
+        extra_small=position_extra_decay.reshape(-1, BLOCK),
         skip_ref=head_skip_weight,
-        value_tap_ref=value_kernel_taps.reshape(-1, BLOCK),
-        key_tap_ref=key_query_kernel,
-        head_gain_ref=head_norm_gain,
+        value_tap_small=value_kernel_taps.reshape(-1, BLOCK),
+        key_tap_small=key_query_kernel,
+        head_gain_small=head_norm_gain,
         matrix_hbm=output_matrix,
-        expert_gain_ref=expert_norm_gain[None],
-        choice_ref=token_expert_choice.T,
-        share_ref=expert_output_weight.T,
+        expert_gain_small=expert_norm_gain[None],
+        choice_small=token_expert_choice.T,
+        share_small=expert_output_weight.T,
         expert_gate_hbm=expert_gate_weight,
         expert_up_hbm=expert_up_weight,
         expert_down_hbm=expert_down_weight,

time: 223 us -> 221 us (level)
  no operation moved by 1% of the time
where the time goes in v4:
time: 221 us
  Pallas kernels  219 us (99%)
    pallas_call x1, Pallas kernels, layer(): pl.pallas_call(functools.partial(layer_kernel, dims, names), out_shape=ja...  219 us

profile of v4, /device:TPU:513, one launch (start us, length us, event | category | flops | bytes accessed | tf_op | source)
XLA Modules:
  0.0 221.2 jit_solution(10502789071616144065)
XLA Ops:
  0.0 219.3 %layer.1 = bf16[128,2048]{1,0:T(8,128)(2,1)} custom-call(bf16[128,2048]{1,0:T(8,128)(2,1)} %refs_0_.1, bf16[2048,128]{1,0:T(8,128)(2,1)} %bitcast.8, bf16[2048,128]{1,0:T(8,128)(2,1)} %bitcast.9, bf16[1024,384]{1,0:T(8,128)(2,1)} %refs_3_.1, bf16[2,2,1024]{2,1,0:T(2,128)(2,1)} %bitcast.10, f32[2,2]{1,0:T(2,128)} %refs_5_.1, f32[2,2]{1,0:T(2,128)} %refs_6_.1, ...), custom_call_target="tpu_custom_call" | custom-call | tf_op jit(solution)/shard_map/layer/pallas_call | solution.py:1161
  219.3 1.9 copy.21

commit v5 on v4

--- a/solution.py
+++ b/solution.py
@@ -56,7 +56,12 @@
         return right if way == 0 else left
 
     barrier = pltpu.get_barrier_semaphore()
-    peers = [{"tp": column(i)} for i in range(1, columns)] + [{"sp": place(i)} for i in range(1, places)]
+    peers = sorted(
+        [(min(i, columns - i), {"tp": column(i)}) for i in range(1, columns)]
+        + [(min(i, places - i) / 2, {"sp": place(i)}) for i in range(1, places)],
+        key=lambda peer: -peer[0],
+    )
+    peers = [device for _, device in peers]
     for device in peers:
         pl.semaphore_signal(barrier, inc=1, device_id=device, device_id_type=MESH)
 
@@ -80,7 +85,7 @@
         (r.residual_hbm, r.residual_in),
     ]
     loads = [pltpu.make_async_copy(a, b, r.load_sem.at[n]) for n, (a, b) in enumerate(loads)]
-    for load in loads[:2] + list(small.values()) + loads[2:]:
+    for load in loads[:2] + list(small.values()) + loads[2:4]:
         load.start()
     for name in ("choice_small", "share_small"):
         small[name].wait()
@@ -204,6 +209,8 @@
                 waiting.remove(step)
                 (serve_ring if step[0] == "x" else serve_grid)(step[1])
 
+    for load in loads[4:]:
+        load.start()
     for t in range(dims.tiles):
         span = pl.ds(t * 128, 128)
         for n, weight in enumerate((r.expert_gate_hbm, r.expert_up_hbm)):
@@ -507,18 +514,15 @@
             r.acc_s[:, span] = part if first else r.acc_s[:, span] + part
 
     serve(*dims.serving[3])
-    serve(*[step for step in waiting if step[0] == "y"])
+    serve(*list(waiting))
     heads_total = remote(
         r.mixed_s.at[most_columns], r.heads_in.at[most_columns], r.head_send.at[0], r.head_recv.at[0], right
     )
     heads_total.wait_recv()
-    remote(pass_totals[1], pass_totals[1], r.pass_send.at[1], r.pass_recv.at[1], mate).wait_recv()
-    for block in range(columns):
-        product(block, ring_part, width, block == 0)
-    serve(*list(waiting))
-    remote(pass_totals[0], pass_totals[0], r.pass_send.at[0], r.pass_recv.at[0], mate).wait_recv()
-    for block in range(columns):
-        product(block, 0, ring_part, block == 0)
+    for which, (low_lane, high_lane) in enumerate(((0, ring_part), (ring_part, width))):
+        remote(pass_totals[which], pass_totals[which], r.pass_send.at[which], r.pass_recv.at[which], mate).wait_recv()
+        for block in range(columns):
+            product(block, low_lane, high_lane, block == 0)
 
     stream = (r.residual_in[...].astype(f32) + r.acc_s[...]).astype(bf16)
     r.stream_s[...] = stream
@@ -640,8 +644,6 @@
                     offset, :, q * lanes_of + c, :
                 ].astype(bf16)
 
-    route(0)
-
     def token_event(k):
         for q in range(thin):
             came = r.tokens.at[pl.ds(0, 2 if k < half else 1), 0, :, pl.ds(0, 128)]
@@ -649,9 +651,6 @@
             for way in range(2):
                 if k < far(way, q):
                     token_ring(way, k, q, column(-k if way == 0 else k)).start()
-        if k < half:
-            route(columns - k)
-        route(k)
 
     def chunk_ring(way, step, p, col):
         here = r.chunks.at[col, p, pl.ds(0, slots), :]
@@ -699,16 +698,15 @@
         view = pass_totals[which]
         remote(view, view, r.pass_send.at[which], r.pass_recv.at[which], mate).wait_send()
 
-    for step in dims.opening:
-        if step > 0:
-            token_event(step)
-        elif -step < direct:
-            start_piece(-step)
-    start_over()
-
     def offset_of(n):
-        k = lax.div(n + 1, 2)
+        k = (n + 1) // 2 if isinstance(n, int) else lax.div(n + 1, 2)
+        if isinstance(n, int):
+            return (columns - k) % columns if n % 2 else k
         return jnp.where(lax.rem(n, 2) == 1, lax.rem(columns - k, columns), k)
+
+    opening = {"token": token_event, "piece": start_piece, "route": lambda n: route(offset_of(n)), "over": lambda n: start_over()}
+    for kind, n in dims.opening:
+        opening[kind](n)
 
     def unit(n, t):
         offset = offset_of(n)
@@ -827,6 +825,8 @@
                     else:
                         pl.when(k < far(way, p))(start)
 
+            if k == 1 and dims.routed < columns:
+                pl.when(p < columns - dims.routed)(lambda: route(offset_of(p + dims.routed)))
             if last > first:
                 units(
                     first + lax.div(p * (last - first), direct), first + lax.div((p + 1) * (last - first), direct)
@@ -1019,12 +1019,22 @@
     tiles, total = units // 128, places * main + over
     ring_part = width * RING_SHARE // 16 // 128 * 128
     schedule = (0, 0, 1, 5, 7) if half == 4 else (0,) * half + (columns - 1,)
-    opening = (1, 0, 2, -1, -2, 3, -3, -4, 4, -5) if half == 4 else (*range(1, half + 1), *range(0, -direct, -1))
+    if half == 4:
+        opening = "token1 piece0 piece1 token2 piece2 route0 piece3 token3 route1 piece4 route2 token4 piece5 over0"
+    else:
+        opening = " ".join(
+            [f"token{n}" for n in range(1, half + 1)]
+            + [f"piece{n}" for n in range(direct)]
+            + [f"route{n}" for n in range(columns)]
+            + ["over0"]
+        )
+    opening = [(step[:-1], int(step[-1])) for step in opening.split()]
+    routed = sum(kind == "route" for kind, _ in opening)
     serving = [
         [("x", 0)],
         [("x", 1)],
         [("x", 2)],
-        [("x", 3), ("y", 0), ("y", 1), ("y", 2), ("x", 4), ("y", 3), ("y", 4), ("y", 5), ("y", 6), ("x", 5)],
+        [("x", 3), ("y", 0), ("y", 1), ("y", 2), ("x", 4), ("y", 3), ("y", 4), ("y", 5), ("x", 5), ("x", 6), ("y", 6)],
     ]
     low, high = (0, (direct + 1) // 2), ((direct + 1) // 2, direct)
     groups = [high, low]
@@ -1055,7 +1065,7 @@
         closing += [("finish", None, group) for group in groups]
     dims = types.SimpleNamespace(
         places=places, columns=columns, width=width, main=main, over=over, pieces=pieces, direct=direct, tiles=tiles,
-        schedule=schedule, opening=opening, small=small, groups=groups, order=(low, high), closing=closing, ring_part=ring_part, serving=serving,
+        schedule=schedule, opening=opening, routed=routed, small=small, groups=groups, order=(low, high), closing=closing, ring_part=ring_part, serving=serving,
     )
     packed = STATE_ONE + STATE_TWO
     square = (blocks, 2, BLOCK, BLOCK)

time: 221 us -> 220 us (level)
  no operation moved by 1% of the time
where the time goes in v5:
time: 220 us
  Pallas kernels  218 us (99%)
    pallas_call x1, Pallas kernels, layer(): pl.pallas_call(functools.partial(layer_kernel, dims, names), out_shape=ja...  218 us

profile of v5, /device:TPU:513, one launch (start us, length us, event | category | flops | bytes accessed | tf_op | source)
XLA Modules:
  0.0 219.9 jit_solution(14034343027768019133)
XLA Ops:
  0.0 218.0 %layer.1 = bf16[128,2048]{1,0:T(8,128)(2,1)} custom-call(bf16[128,2048]{1,0:T(8,128)(2,1)} %refs_0_.1, bf16[2048,128]{1,0:T(8,128)(2,1)} %bitcast.8, bf16[2048,128]{1,0:T(8,128)(2,1)} %bitcast.9, bf16[1024,384]{1,0:T(8,128)(2,1)} %refs_3_.1, bf16[2,2,1024]{2,1,0:T(2,128)(2,1)} %bitcast.10, f32[2,2]{1,0:T(2,128)} %refs_5_.1, f32[2,2]{1,0:T(2,128)} %refs_6_.1, ...), custom_call_target="tpu_custom_call" | custom-call | tf_op jit(solution)/shard_map/layer/pallas_call | solution.py:1171
  218.0 1.9 copy.21

commit v6 on v5

--- a/solution.py
+++ b/solution.py
@@ -18,7 +18,7 @@
 PIECE = 256
 HEADS = 4
 RING_SHARE = 7
-VMEM_LIMIT = 67043328
+VMEM_LIMIT = 61600000
 
 
 def remote(src, dst, send, recv, device):
@@ -70,6 +70,7 @@
         for n, name in enumerate(dims.small)
     }
     ring_part, slab = dims.ring_part, rows // chips
+    rim_rows, positions = 16, blocks * rows
     mine = pl.multiple_of(core * rows, rows)
 
     def slab_rows(y):
@@ -79,8 +80,8 @@
     loads = [
         (r.matrix_hbm.at[0], r.matrix.at[0, pl.ds(0, rows), :]),
         (r.matrix_hbm.at[1], r.matrix.at[0, pl.ds(rows, rows), :]),
-        (r.value_hbm, r.value_in),
-        (r.keys_hbm, r.keys_in),
+        (r.value_hbm, r.value_in.at[pl.ds(rim_rows, 2 * positions), :]),
+        (r.keys_hbm, r.keys_in.at[pl.ds(rim_rows, positions), :]),
         (r.gate_hbm, r.gate_in),
         (r.residual_hbm, r.residual_in),
     ]
@@ -142,18 +143,20 @@
 
     for load in loads[2:4]:
         load.wait()
-    rim_rows = 16
-    positions = blocks * rows
     rims = [
         remote(
-            r.value_in.at[pl.ds(2 * positions - rim_rows, rim_rows), :],
-            r.value_rim,
+            r.value_in.at[pl.ds(2 * positions, rim_rows), :],
+            r.value_in.at[pl.ds(0, rim_rows), :],
             r.rim_send.at[0],
             r.rim_recv.at[0],
             following,
         ),
         remote(
-            r.keys_in.at[pl.ds(positions - rim_rows, rim_rows), :], r.keys_rim, r.rim_send.at[1], r.rim_recv.at[1], following
+            r.keys_in.at[pl.ds(positions, rim_rows), :],
+            r.keys_in.at[pl.ds(0, rim_rows), :],
+            r.rim_send.at[1],
+            r.rim_recv.at[1],
+            following,
         ),
     ]
     for rim in rims:
@@ -266,8 +269,6 @@
         high = table[pl.ds(HEADS * k + 2 * g + 1, 1), :]
         return jnp.where(first_head[0:1], low, high)
 
-    r.value_wide[rim_rows:, :] = r.value_in[...].astype(f32)
-    r.keys_wide[rim_rows:, :] = r.keys_in[...].astype(f32)
     taps = r.value_tap_ref.shape[0] // 2
     value_tap = r.value_tap_ref[...].astype(f32)
     key_tap = r.key_tap_ref[...].astype(f32)
@@ -275,14 +276,14 @@
     tap_rows = [jnp.where(even, value_tap[2 * j : 2 * j + 1], value_tap[2 * j + 1 : 2 * j + 2]) for j in range(taps)]
 
     def states_of(k):
-        window = r.value_wide[pl.ds(pl.multiple_of(k * 2 * rows, 2 * rows), 2 * rows + rim_rows), :]
+        window = r.value_in[pl.ds(pl.multiple_of(k * 2 * rows, 2 * rows), 2 * rows + rim_rows), :].astype(f32)
         total = jnp.zeros((2 * rows, rows), f32)
         for j in range(taps):
             start = rim_rows - 2 * (taps - 1 - j)
             total = total + window[start : start + 2 * rows] * tap_rows[j]
         r.conv_wide[...] = silu(total).astype(bf16).astype(f32)
-        window = r.keys_wide[pl.ds(pl.multiple_of(k * rows, rows), rows + rim_rows), :]
-        total = jnp.zeros((rows, r.keys_wide.shape[1]), f32)
+        window = r.keys_in[pl.ds(pl.multiple_of(k * rows, rows), rows + rim_rows), :].astype(f32)
+        total = jnp.zeros((rows, r.keys_in.shape[1]), f32)
         for j in range(taps):
             start = rim_rows - (taps - 1 - j)
             total = total + window[start : start + rows] * key_tap[j : j + 1]
@@ -310,8 +311,8 @@
     for rim in rims:
         rim.wait_recv()
     opening = me_s == 0
-    r.value_wide[0:rim_rows, :] = jnp.where(opening, 0.0, r.value_rim[...].astype(f32))
-    r.keys_wide[0:rim_rows, :] = jnp.where(opening, 0.0, r.keys_rim[...].astype(f32))
+    for table in (r.value_in, r.keys_in):
+        table[0:rim_rows, :] = jnp.where(opening, 0.0, table[0:rim_rows, :].astype(f32)).astype(bf16)
     states_of(0)
 
     packed = STATE_TWO + STATE_ONE
@@ -954,9 +955,6 @@
     left_by_now(r.xover_back.at[:, most_places], r.xover_send.at[1], r.xover_recv.at[1, 0])
     left_by_now(r.chunks.at[most_columns, pl.ds(0, direct)], r.sum_send.at[0], r.sum_recv.at[0, 0, 0])
     token_round(half - 1)
-    def write_out(span):
-        return pltpu.make_async_copy(r.out_s.at[:, span], r.out_ref.at[:, span], r.done_sem.at[0])
-
     def back_arrived(p):
         most = pl.ds(0, (places - 1) * main)
         return remote(
@@ -967,8 +965,7 @@
         back_arrived(p).wait_recv()
         span = pl.ds(pl.multiple_of(p * PIECE, PIECE), PIECE)
         value = weighted(me_x, r.returned[p])
-        r.out_s[:, span] = (r.stream_s[:, span].astype(f32) + value).astype(bf16)
-        write_out(span).start()
+        r.out_ref[:, span] = (r.stream_s[:, span].astype(f32) + value).astype(bf16)
         return carry
 
     def combine_group(n, group):
@@ -992,15 +989,13 @@
             token_hop(way, 1, q).wait_recv()
             value = value + r.xsums[way, 0, q].astype(f32)
         span = slice(direct * PIECE + q * 128, direct * PIECE + (q + 1) * 128)
-        r.out_s[:, span] = (r.stream_s[:, span].astype(f32) + value).astype(bf16)
-
-    write_out(pl.ds(direct * PIECE, extra * PIECE)).start()
+        r.out_ref[:, span] = (r.stream_s[:, span].astype(f32) + value).astype(bf16)
+
     combine_group(dims.groups.index(dims.order[1]), dims.order[1])
 
     left_by_now(r.over_back.at[:, most_places], r.over_send.at[1], r.over_recv.at[1])
     left_by_now(r.tokens.at[most_columns], r.xsum_send.at[0], r.xsum_recv.at[0, 0, 0])
     left_by_now(r.totals.at[:, most_lines, :], r.back_send.at[0], r.back_recv.at[0])
-    pltpu.make_async_copy(r.out_s, r.out_ref, r.done_sem.at[0]).wait()
 
 
 def layer(places, columns, **given):
@@ -1020,15 +1015,11 @@
     ring_part = width * RING_SHARE // 16 // 128 * 128
     schedule = (0, 0, 1, 5, 7) if half == 4 else (0,) * half + (columns - 1,)
     if half == 4:
-        opening = "token1 piece0 piece1 token2 piece2 route0 piece3 token3 route1 piece4 route2 token4 piece5 over0"
+        opening = [("token", 1), ("piece", 0), ("piece", 1), ("token", 2), ("piece", 2), ("route", 0), ("piece", 3)]
+        opening += [("token", 3), ("route", 1), ("piece", 4), ("route", 2), ("token", 4), ("piece", 5), ("over", 0)]
     else:
-        opening = " ".join(
-            [f"token{n}" for n in range(1, half + 1)]
-            + [f"piece{n}" for n in range(direct)]
-            + [f"route{n}" for n in range(columns)]
-            + ["over0"]
-        )
-    opening = [(step[:-1], int(step[-1])) for step in opening.split()]
+        opening = [("token", n) for n in range(1, half + 1)] + [("piece", n) for n in range(direct)]
+        opening += [("route", n) for n in range(columns)] + [("over", 0)]
     routed = sum(kind == "route" for kind, _ in opening)
     serving = [
         [("x", 0)],
@@ -1076,13 +1067,9 @@
     scratch = {name[:-5] + "ref": pltpu.VMEM(given[name].shape, given[name].dtype) for name in small}
     scratch |= dict(
         residual_in=vmem(rows, width),
-        value_in=vmem(2 * positions, BLOCK),
+        value_in=vmem(2 * positions + 16, BLOCK),
         gate_in=vmem(2 * positions, BLOCK),
-        keys_in=vmem(positions, lanes),
-        value_rim=vmem(16, BLOCK),
-        keys_rim=vmem(16, lanes),
-        value_wide=vmem(2 * positions + 16, BLOCK, dtype=f32),
-        keys_wide=vmem(positions + 16, lanes, dtype=f32),
+        keys_in=vmem(positions + 16, lanes),
         gate_wide=vmem(2 * BLOCK, BLOCK, dtype=f32),
         conv_wide=vmem(2 * BLOCK, BLOCK, dtype=f32),
         x_s=vmem(*square),
@@ -1110,7 +1097,6 @@
         matrix=vmem(columns, 2 * BLOCK, width),
         acc_s=vmem(rows, width, dtype=f32),
         stream_s=vmem(rows, width),
-        out_s=vmem(rows, width),
         tables=vmem(columns, 8, rows, dtype=f32),
         put=vmem(columns, total, rows),
         pick=vmem(columns, 2, rows, total),
@@ -1139,7 +1125,6 @@
         returned=vmem(direct, total, PIECE),
         load_sem=dma(6),
         weight_sem=dma(2),
-        done_sem=dma(1),
         small_sem=dma(len(small)),
     )
     steps = (2, half)
@@ -1170,9 +1155,9 @@
     names = [*given, "out_ref", *scratch]
     return pl.pallas_call(
         functools.partial(layer_kernel, dims, names),
-        out_shape=jax.ShapeDtypeStruct((rows, width), bf16),
+        out_shape=pltpu.VMEM((rows, width), bf16),
         in_specs=in_specs,
-        out_specs=pl.BlockSpec(memory_space=pl.ANY),
+        out_specs=pl.BlockSpec(memory_space=pltpu.VMEM),
         scratch_shapes=list(scratch.values()),
         compiler_params=pltpu.CompilerParams(
             collective_id=0, has_side_effects=True, vmem_limit_bytes=VMEM_LIMIT

time: 220 us -> 218 us (level)
  no operation moved by 1% of the time
where the time goes in v6:
time: 218 us
  Pallas kernels  217 us (100%)
    pallas_call x1, Pallas kernels, layer(): pl.pallas_call(functools.partial(layer_kernel, dims, names), out_shape=pl...  217 us

profile of v6, /device:TPU:513, one launch (start us, length us, event | category | flops | bytes accessed | tf_op | source)
XLA Modules:
  0.0 218.0 jit_solution(7868889540579479922)
XLA Ops:
  0.0 217.2 %layer.1 = bf16[128,2048]{1,0:T(8,128)(2,1)S(1)} custom-call(bf16[128,2048]{1,0:T(8,128)(2,1)} %refs_0_.1, bf16[2048,128]{1,0:T(8,128)(2,1)} %bitcast.8, bf16[2048,128]{1,0:T(8,128)(2,1)} %bitcast.9, bf16[1024,384]{1,0:T(8,128)(2,1)} %refs_3_.1, bf16[2,2,1024]{2,1,0:T(2,128)(2,1)} %bitcast.10, f32[2,2]{1,0:T(2,128)} %refs_5_.1, f32[2,2]{1,0:T(2,128)} %refs_6_.1, ...), custom_call_target="tpu_custom_call" | custom-call | tf_op jit(solution)/shard_map/layer/pallas_call | solution.py:1156
  217.2 0.8 copy.21

commit v7 on v6

--- a/solution.py
+++ b/solution.py
@@ -58,7 +58,7 @@
     barrier = pltpu.get_barrier_semaphore()
     peers = sorted(
         [(min(i, columns - i), {"tp": column(i)}) for i in range(1, columns)]
-        + [(min(i, places - i) / 2, {"sp": place(i)}) for i in range(1, places)],
+        + [(min(i, places - i) / 2, {"sp": place(i)}) for i in range(1, places) if i % 2 == 0 or i in (1, places - 1)],
         key=lambda peer: -peer[0],
     )
     peers = [device for _, device in peers]
@@ -1015,8 +1015,8 @@
     ring_part = width * RING_SHARE // 16 // 128 * 128
     schedule = (0, 0, 1, 5, 7) if half == 4 else (0,) * half + (columns - 1,)
     if half == 4:
-        opening = [("token", 1), ("piece", 0), ("piece", 1), ("token", 2), ("piece", 2), ("route", 0), ("piece", 3)]
-        opening += [("token", 3), ("route", 1), ("piece", 4), ("route", 2), ("token", 4), ("piece", 5), ("over", 0)]
+        opening = [("token", 1), ("piece", 0), ("token", 2), ("piece", 1), ("piece", 2), ("token", 3), ("piece", 3)]
+        opening += [("route", 0), ("piece", 4), ("token", 4), ("piece", 5), ("route", 1), ("route", 2), ("over", 0)]
     else:
         opening = [("token", n) for n in range(1, half + 1)] + [("piece", n) for n in range(direct)]
         opening += [("route", n) for n in range(columns)] + [("over", 0)]
@@ -1041,8 +1041,8 @@
             ("short", 2, low),
             ("token", 0, None),
             ("long", 3, high),
+            ("short", 2, high),
             ("finish", None, low),
-            ("short", 2, high),
             ("token", 1, None),
             ("finish", None, high),
             ("token", 2, None),

time: 218 us -> 218 us (level)
  no operation moved by 1% of the time
where the time goes in v7:
time: 218 us; the launch traced here: 217 us
  Pallas kernels  217 us (100%)
    pallas_call x1, Pallas kernels, layer(): pl.pallas_call(functools.partial(layer_kernel, dims, names), out_shape=pl...  217 us

profile of v7, /device:TPU:513, one launch (start us, length us, event | category | flops | bytes accessed | tf_op | source)
XLA Modules:
  0.0 217.5 jit_solution(17412794646719494875)
XLA Ops:
  0.0 216.7 %layer.1 = bf16[128,2048]{1,0:T(8,128)(2,1)S(1)} custom-call(bf16[128,2048]{1,0:T(8,128)(2,1)} %refs_0_.1, bf16[2048,128]{1,0:T(8,128)(2,1)} %bitcast.8, bf16[2048,128]{1,0:T(8,128)(2,1)} %bitcast.9, bf16[1024,384]{1,0:T(8,128)(2,1)} %refs_3_.1, bf16[2,2,1024]{2,1,0:T(2,128)(2,1)} %bitcast.10, f32[2,2]{1,0:T(2,128)} %refs_5_.1, f32[2,2]{1,0:T(2,128)} %refs_6_.1, ...), custom_call_target="tpu_custom_call" | custom-call | tf_op jit(solution)/shard_map/layer/pallas_call | solution.py:1156
  216.7 0.8 copy.21

commit v8 on v7

--- a/solution.py
+++ b/solution.py
@@ -58,10 +58,18 @@
     barrier = pltpu.get_barrier_semaphore()
     peers = sorted(
         [(min(i, columns - i), {"tp": column(i)}) for i in range(1, columns)]
-        + [(min(i, places - i) / 2, {"sp": place(i)}) for i in range(1, places) if i % 2 == 0 or i in (1, places - 1)],
+        + [(min(i, places - i) / 2, {"sp": place(i)}) for i in sorted({1, 2, places - 2, places - 1})],
         key=lambda peer: -peer[0],
     )
     peers = [device for _, device in peers]
+    later = 0
+    for n in range(2, chips - 1):
+        later = later + jnp.where(me_y + n < chips, 1, 0)
+
+        @pl.when(me_y + n >= chips)
+        def _():
+            pl.semaphore_signal(barrier, inc=1, device_id=peer(n), device_id_type=MESH)
+
     for device in peers:
         pl.semaphore_signal(barrier, inc=1, device_id=device, device_id_type=MESH)
 
@@ -96,7 +104,7 @@
 
     for load in loads[:2]:
         load.wait()
-    pl.semaphore_wait(barrier, len(peers))
+    pl.semaphore_wait(barrier, len(peers) + later)
 
     def matrix_block(way, event, k, sub):
         piece = ((event % 2) ^ way) * 2 + sub

time: 218 us -> 217 us (level)
  no operation moved by 1% of the time
where the time goes in v8:
time: 217 us
  Pallas kernels  216 us (100%)
    pallas_call x1, Pallas kernels, layer(): pl.pallas_call(functools.partial(layer_kernel, dims, names), out_shape=pl...  216 us

profile of v8, /device:TPU:513, one launch (start us, length us, event | category | flops | bytes accessed | tf_op | source)
XLA Modules:
  0.0 217.3 jit_solution(14673866693655155853)
XLA Ops:
  0.0 216.4 %layer.1 = bf16[128,2048]{1,0:T(8,128)(2,1)S(1)} custom-call(bf16[128,2048]{1,0:T(8,128)(2,1)} %refs_0_.1, bf16[2048,128]{1,0:T(8,128)(2,1)} %bitcast.8, bf16[2048,128]{1,0:T(8,128)(2,1)} %bitcast.9, bf16[1024,384]{1,0:T(8,128)(2,1)} %refs_3_.1, bf16[2,2,1024]{2,1,0:T(2,128)(2,1)} %bitcast.10, f32[2,2]{1,0:T(2,128)} %refs_5_.1, f32[2,2]{1,0:T(2,128)} %refs_6_.1, ...), custom_call_target="tpu_custom_call" | custom-call | tf_op jit(solution)/shard_map/layer/pallas_call | solution.py:1164
  216.5 0.8 copy.21
